TPU v7x, 32 devices: a whole 2x2x4 slice. The times are simulated.
32 devices in a mesh: sp: 8 (over z, y), tp: 4 (over x, core).
Axes of the slice: x: 2, y: 2, z: 4, core: 2. Of those that a mesh axis runs over, the one named last changes fastest.
Arguments:
- mixer_input: bfloat16 [2048, 1024], P('sp', 'tp'), may hold values from -6 to 6
- retention: float32 [64, 2048], P('tp', 'sp'), may hold values from -1 to 0
- decay_real: float32 [64, 64], P('tp'), may hold values from -0.7 to -0.3
- decay_freq: float32 [64, 64], P('tp'), may hold values from 0 to 26
- log_step: float32 [64], P('tp')
- input_real: float32 [64, 64, 16], P('tp')
- input_imag: float32 [64, 64, 16], P('tp')
- readout_real: float32 [64, 16, 64], P('tp'), may hold values from -0.5 to 0.5
- readout_imaginary: float32 [64, 16, 64], P('tp'), may hold values from -0.5 to 0.5
- skip_weight: float32 [64, 16], P('tp'), may hold values from -4 to 4
- norm_gain: float32 [1024], replicated, may hold values from 0.1 to 1.9
- projection: bfloat16 [1024, 2048], P('tp'), may hold values from -0.1875 to 0.1875
- residual: bfloat16 [2048, 2048], P(('sp', 'tp')), may hold values from -6 to 6
- mix_gain: float32 [2048], replicated, may hold values from 0.1 to 1.9
- routes: int32 [2048, 2], P(('sp', 'tp')), may hold values from 0 to 7, all different within a row; in each aligned block of 64 rows (0 to 63, 64 to 127, ...) at most 32 rows name the same one
- route_weight: float32 [2048, 2], P(('sp', 'tp')), may hold values from 0.5 to 2
- expert_gate: bfloat16 [8, 2048, 512], P('sp'), may hold values from -0.125 to 0.125
- expert_up: bfloat16 [8, 2048, 512], P('sp'), may hold values from -0.125 to 0.125
- expert_down: bfloat16 [8, 512, 2048], P('sp'), may hold values from -0.25 to 0.25
- final_gain: float32 [2048], replicated, may hold values from 0.1 to 1.9
Outputs:
- layer_out: bfloat16 [2048, 2048], P(('sp', 'tp'))
Inputs may be any that keep to these rules, and one draw needn't show every extreme that they name: `routes`: in each aligned block of 64 rows no expert is named by more than 32 rows, and in some blocks one is named by exactly 32 rows; each row names 2 different experts.
All inputs are finite; a program needn't handle non-finite values.
Results may differ from a plain program's by a relative error of at most 0.017.
Values may be sent and summed in bfloat16 or wider, within the bound.
No kernel may reach another device: no remote copies, remote signals or barrier semaphores. Data moves between devices by JAX's collectives and lax.ppermute only.
A program may use at most 64 MiB of HBM per device.

v0:
```python
import jax
import jax.numpy as jnp
from jax import lax
from jax.sharding import PartitionSpec as P

PICKS = 2
MIX_WIDTH = 1024


deep_alpha = 2.0**0.25
highest_precision = lax.Precision.HIGHEST
span_length = 16


def prefix(value, axis, join, neutral):
    count, mine = (lax.axis_size(axis), lax.axis_index(axis))
    pieces = jax.tree.map(lambda part: lax.all_gather(part, axis), value)
    subtotal = jax.tree.map(
        lambda part, zero: jnp.full_like(part, 0) + jnp.asarray(zero, part.dtype), value, neutral
    )

    def step(position, subtotal):
        longer = join(subtotal, jax.tree.map(lambda part: part[position], pieces))
        return jax.tree.map(lambda new, old: jnp.where(position < mine, new, old), longer, subtotal)

    return lax.fori_loop(0, count - 1, step, subtotal)


def input_factor(decay_real, decay_freq, log_step):
    stride = jnp.exp(log_step)[:, None]
    growth = decay_real * stride
    turning = decay_freq * stride
    upper_real = jnp.expm1(growth) * jnp.cos(turning) - 2.0 * jnp.sin(0.5 * turning) ** 2
    upper_imag = jnp.exp(growth) * jnp.sin(turning)
    denominator = decay_real * decay_real + decay_freq * decay_freq
    factor_real = (upper_real * decay_real + upper_imag * decay_freq) / denominator
    factor_imag = (upper_imag * decay_real - upper_real * decay_freq) / denominator
    return (growth, turning, factor_real, factor_imag)


def layer_norm(values, scales):
    centered = values - jnp.mean(values, axis=-1, keepdims=True)
    variance = jnp.mean(centered * centered, axis=-1, keepdims=True)
    return centered * lax.rsqrt(variance + 1e-05) * scales


def chain_combine(earlier, later):
    return (
        earlier[0] * later[0] - earlier[1] * later[1],
        earlier[0] * later[1] + earlier[1] * later[0],
        later[0] * earlier[2] - later[1] * earlier[3] + later[2],
        later[0] * earlier[3] + later[1] * earlier[2] + later[3],
    )


def times_complex(left_real, left_imag, right_real, right_imag):
    return (
        left_real * right_real - left_imag * right_imag,
        left_real * right_imag + left_imag * right_real,
    )


def read_state(state_real_part, state_imaginary, readout_real, readout_imaginary):
    leading_term = jnp.einsum(
        "motx,tkx->motk", state_real_part, readout_real, precision=highest_precision
    )
    return leading_term - jnp.einsum(
        "motx,tkx->motk", state_imaginary, readout_imaginary, precision=highest_precision
    )


def local(
    mixer_input,
    retention,
    decay_real,
    decay_freq,
    log_step,
    input_real,
    input_imag,
    readout_real,
    readout_imaginary,
    skip_weight,
    norm_gain,
    projection,
    residual,
    mix_gain,
    routes,
    route_weight,
    expert_gate,
    expert_up,
    expert_down,
    final_gain,
):
    token_count = mixer_input.shape[0]
    group_count = decay_real.shape[0]
    channel_count = input_real.shape[2]
    span_count = token_count // span_length
    growth, turning, factor_real, factor_imag = input_factor(decay_real, decay_freq, log_step)
    bar_real = factor_real[:, :, None] * input_real - factor_imag[:, :, None] * input_imag
    bar_imag = factor_real[:, :, None] * input_imag + factor_imag[:, :, None] * input_real
    inputs = mixer_input.astype(jnp.float32).reshape(token_count, group_count, channel_count)
    drive_real = jnp.einsum("tgc,gpc->tgp", inputs, bar_real, precision=highest_precision)
    drive_imag = jnp.einsum("tgc,gpc->tgp", inputs, bar_imag, precision=highest_precision)
    drive_real = drive_real.reshape(span_count, span_length, group_count, -1)
    drive_imag = drive_imag.reshape(span_count, span_length, group_count, -1)
    held_log = jnp.cumsum(
        jnp.transpose(retention).reshape(span_count, span_length, group_count), axis=1
    )
    offsets = jnp.arange(1, span_length + 1, dtype=jnp.float32)[:, None, None]
    log_size = offsets * growth + held_log[:, :, :, None]
    turn_angle = offsets * turning
    grown_size = jnp.exp(log_size)
    shrunk = jnp.exp(-log_size)
    prefix_real = grown_size * jnp.cos(turn_angle)
    prefix_imag = grown_size * jnp.sin(turn_angle)
    weighted_real, weighted_imag = times_complex(
        drive_real, drive_imag, shrunk * jnp.cos(turn_angle), -shrunk * jnp.sin(turn_angle)
    )
    inner_real, inner_imag = times_complex(
        prefix_real,
        prefix_imag,
        jnp.cumsum(weighted_real, axis=1),
        jnp.cumsum(weighted_imag, axis=1),
    )
    scanned = lax.associative_scan(
        chain_combine,
        (prefix_real[:, -1], prefix_imag[:, -1], inner_real[:, -1], inner_imag[:, -1]),
        axis=0,
    )
    ones_row = jnp.ones_like(scanned[0][:1])
    zeros_row = jnp.zeros_like(ones_row)
    enter_decay_real = jnp.concatenate([ones_row, scanned[0][:-1]], axis=0)
    enter_decay_imag = jnp.concatenate([zeros_row, scanned[1][:-1]], axis=0)
    enter_state_real = jnp.concatenate([zeros_row, scanned[2][:-1]], axis=0)
    enter_state_imag = jnp.concatenate([zeros_row, scanned[3][:-1]], axis=0)
    identity = (
        jnp.ones_like(growth),
        jnp.zeros_like(growth),
        jnp.zeros_like(growth),
        jnp.zeros_like(growth),
    )
    carried = prefix(
        (scanned[0][-1], scanned[1][-1], scanned[2][-1], scanned[3][-1]),
        "sp",
        chain_combine,
        identity,
    )
    skip_term = (skip_weight * inputs).reshape(span_count, span_length, group_count, channel_count)
    carry_real, carry_imag = times_complex(
        enter_decay_real, enter_decay_imag, carried[2], carried[3]
    )
    state_real_part, state_imaginary = times_complex(
        prefix_real,
        prefix_imag,
        (enter_state_real + carry_real)[:, None],
        (enter_state_imag + carry_imag)[:, None],
    )
    readout_result = read_state(
        inner_real + state_real_part, inner_imag + state_imaginary, readout_real, readout_imaginary
    )
    mixed_seq = (
        jax.nn.gelu(readout_result + skip_term).astype(jnp.bfloat16).reshape(token_count, -1)
    )
    row_count = token_count // lax.axis_size("tp")
    whole_rows = lax.all_to_all(mixed_seq, "tp", split_axis=0, concat_axis=1, tiled=True)
    whole_float = whole_rows.astype(jnp.float32)
    squares = jnp.sum(whole_float * whole_float, axis=1)
    scaled = (whole_float * norm_gain).astype(jnp.bfloat16)
    summed = jnp.dot(
        scaled,
        lax.all_gather(projection, "tp", axis=0, tiled=True),
        preferred_element_type=jnp.float32,
    )
    mix = summed * lax.rsqrt(squares / MIX_WIDTH + 1e-06)[:, None]
    hidden = layer_norm(deep_alpha * residual.astype(jnp.float32) + mix, mix_gain).astype(
        jnp.bfloat16
    )
    expert_count = lax.axis_size("sp")
    capacity = max(2, 2 * row_count * PICKS // expert_count)
    chosen = routes.reshape(-1)
    onehot = (chosen[:, None] == jnp.arange(expert_count, dtype=jnp.int32)[None, :]).astype(
        jnp.int32
    )
    slot_index = jnp.sum((jnp.cumsum(onehot, axis=0) - 1) * onehot, axis=1)
    target = chosen * capacity + slot_index
    source_row = jnp.full((expert_count * capacity,), row_count, jnp.int32)
    source_row = source_row.at[target].set(jnp.arange(row_count * PICKS, dtype=jnp.int32) // PICKS)
    padded = jnp.concatenate([hidden, jnp.zeros((1, hidden.shape[1]), hidden.dtype)], axis=0)
    outgoing = padded[source_row].reshape(expert_count, capacity, -1)
    received = lax.all_to_all(outgoing, "sp", split_axis=0, concat_axis=0, tiled=True)
    arrived = received.reshape(-1, received.shape[2])
    gate_act = jnp.dot(arrived, expert_gate[0], preferred_element_type=jnp.float32)
    up_act = jnp.dot(arrived, expert_up[0], preferred_element_type=jnp.float32)
    active = (jax.nn.silu(gate_act) * up_act).astype(jnp.bfloat16)
    produced = jnp.dot(active, expert_down[0], preferred_element_type=jnp.float32).astype(
        jnp.bfloat16
    )
    returned = lax.all_to_all(
        produced.reshape(received.shape), "sp", split_axis=0, concat_axis=0, tiled=True
    )
    gathered_rows = returned.reshape(expert_count * capacity, -1)[target].reshape(
        row_count, PICKS, -1
    )
    expert_mix = jnp.sum(route_weight[:, :, None] * gathered_rows.astype(jnp.float32), axis=1)
    layer_out = layer_norm(deep_alpha * hidden.astype(jnp.float32) + expert_mix, final_gain)
    return layer_out.astype(jnp.bfloat16)


def solution(mesh):
    in_specs = (
        P("sp", "tp"),
        P("tp", "sp"),
        P("tp", None),
        P("tp", None),
        P("tp"),
        P("tp", None, None),
        P("tp", None, None),
        P("tp", None, None),
        P("tp", None, None),
        P("tp", None),
        P(),
        P("tp", None),
        P(("sp", "tp"), None),
        P(),
        P(("sp", "tp"), None),
        P(("sp", "tp"), None),
        P("sp", None, None),
        P("sp", None, None),
        P("sp", None, None),
        P(),
    )
    out_specs = P(("sp", "tp"), None)
    return jax.shard_map(local, mesh=mesh, in_specs=in_specs, out_specs=out_specs, check_vma=False)
```

profile of v0, /device:TPU:0, one launch (start us, length us, event | category | flops | bytes accessed | tf_op | source)
XLA Modules:
  0.0 337.1 jit_solution(15495146803152254095)
XLA Ops:
  9.8 2.6 convolution_bitcast_fusion.1
  13.1 3.7 %copy.54 = f32[256,16,64]{2,1,0:T(8,128)} copy(f32[256,16,64]{0,2,1:T(8,128)} %convolution_bitcast_fusion.1) | data formatting | bytes 2097152 | tf_op jit(solution)/shard_map/tgc,gpc->tgp/transpose | solution.py:102
  16.8 2.5 copy.55
  20.9 2.8 fusion.27
  36.5 1.9 pad.110
  50.0 3.0 pad.173
  53.1 3.0 pad.135
  63.3 3.0 pad.268
  66.5 3.1 pad.133
  69.5 3.0 pad.171
  72.6 3.0 pad.270
  75.7 2.0 reshape.138
  77.7 2.8 pad.265
  80.5 2.8 pad.266
  86.1 2.8 pad.117
  89.6 33.6 %all_gather.18 = f32[8,16,64]{2,1,0:T(8,128)} all-gather(f32[1,16,64]{2,1,0:T(8,128)S(1)} %slice_add_fusion.20), channel_id=1, replica_groups=mesh['sp'=8,'tp'=4] {'sp'}, dimensions={0}, use_global_device_ids=true | all-gather | bytes 36864 | tf_op jit(solution)/shard_map/all_gather | solution.py:17
  124.0 32.4 %all_gather.16 = f32[8,16,64]{2,1,0:T(8,128)} all-gather(f32[1,16,64]{2,1,0:T(8,128)S(1)} %slice_add_fusion.21), channel_id=1, replica_groups=mesh['sp'=8,'tp'=4] {'sp'}, dimensions={0}, use_global_device_ids=true | all-gather | bytes 36864 | tf_op jit(solution)/shard_map/all_gather | solution.py:17
  156.4 32.4 %all_gather.15 = f32[8,16,64]{2,1,0:T(8,128)} all-gather(f32[1,16,64]{2,1,0:T(8,128)S(1)} %slice-done), channel_id=1, replica_groups=mesh['sp'=8,'tp'=4] {'sp'}, dimensions={0}, use_global_device_ids=true | all-gather | bytes 36864 | tf_op jit(solution)/shard_map/all_gather | solution.py:17
  188.9 32.9 %all_gather.17 = f32[8,16,64]{2,1,0:T(8,128)} all-gather(f32[1,16,64]{2,1,0:T(8,128)} %slice.679), channel_id=1, replica_groups=mesh['sp'=8,'tp'=4] {'sp'}, dimensions={0}, use_global_device_ids=true | all-gather | bytes 36864 | tf_op jit(solution)/shard_map/all_gather | solution.py:17
  223.4 5.4 %while.16 = (s32[]{:T(128)}, f32[16,64]{1,0:T(8,128)S(1)}, f32[16,64]{1,0:T(8,128)S(1)}, s32[]{:T(128)}, f32[8,16,64]{2,1,0:T(8,128)}, /*index=5*/f32[8,16,64]{2...) while((s32[]{:T(128)}, f32[16,64]{1,0:T(8,128)S(1)}, ...), condition=%wide.region_4.5_spmd.clone, body=%wide.region_3.4_spmd.clone.sunk | while | flops 12292 | bytes 32893 | solution.py:26
  229.8 2.8 fusion.18
  232.6 2.5 fusion.50
  235.2 3.8 %fusion.44 = bf16[16,16,16,16]{3,1,0,2:T(8,128)(2,1)S(1)} fusion(f32[16,16,16,16]{3,2,1,0:T(8,128)S(1)} %copy-done.9, f32[16,16,16,16]{3,2,1,0:T(8,128)S(1)} %fusion.50, f32[16,16,16,64]{3,2,1,0:T(8,128)S(1)} %get-tuple-element.194, f32[16,16]{1,0:T(8,128)S(1)} %copy-done.30, f32[16,16,64]{2,1,0:T(8,128)S(1)} %copy-done.29), kind=kOutput, calls=%fused_computation.54 | convolution fusion | flops 51118080 | bytes 1770496 | tf_op jit(solution)/shard_map/motx,tkx->motk/dot_general | solution.py:64
  241.3 3.3 all-to-all-start
  246.6 2.6 all-to-all-done
  249.5 3.2 fusion.103
  255.0 31.2 %all_to_all.23 = bf16[8,32,2048]{2,1,0:T(8,128)(2,1)S(1)} all-to-all(bf16[8,32,2048]{2,1,0:T(8,128)(2,1)S(1)} %bitcast.118), channel_id=1, replica_groups=mesh['sp'=8,'tp'=4] {'sp'}, dimensions={0} | all-to-all | bytes 2097152 | tf_op jit(solution)/shard_map/all_to_all | solution.py:190
  287.9 4.2 %convolution_convert_fusion = bf16[256,2048]{1,0:T(8,128)(2,1)} fusion(bf16[1,512,2048]{2,1,0:T(8,128)(2,1)S(1)} %copy-done, bf16[256,2048]{1,0:T(8,128)(2,1)} %bitcast.124, bf16[1,2048,512]{2,1,0:T(8,128)(2,1)} %param.39, f32[256,512]{1,0:T(8,128)S(1)} %fusion.48), kind=kOutput, calls=%fused_computation.26 | convolution fusion | flops 1075052544 | bytes 6815744 | tf_op jit(solution)/shard_map/dot_general | solution.py:195
  292.1 3.7 %all-to-all-start.2 = ((bf16[8,32,2048]{2,1,0:T(8,128)(2,1)}), bf16[8,32,2048]{2,1,0:T(8,128)(2,1)S(1)}, u32[]{:S(2)}, u32[]{:S(2)}) async-start(bf16[8,32,2048]{2,1,0:T(8,128)(2,1)} %bitcast.122), calls=%async_computation.2 | async-start | bytes 2097152 | tf_op jit(solution)/shard_map/all_to_all | solution.py:198
  295.9 25.4 %all-to-all-done.2 = bf16[8,32,2048]{2,1,0:T(8,128)(2,1)S(1)} async-done(((bf16[8,32,2048]{2,1,0:T(8,128)(2,1)}), bf16[8,32,2048]{2,1,0:T(8,128)(2,1)S(1)}, u32[]{:S(2)}, u32[]{:S(2)}) %all-to-all-start.2) | async-done | bytes 1048608 | tf_op jit(solution)/shard_map/all_to_all | solution.py:198
  323.0 2.8 reshape.140
  325.8 2.8 multiply_reduce_fusion
  (192 shorter events, 60.9 us)
Async XLA Ops:
  6.5 281.3 %copy-start = (bf16[1,512,2048]{2,1,0:T(8,128)(2,1)S(1)}, bf16[1,512,2048]{2,1,0:T(8,128)(2,1)}, u32[]{:S(2)}) copy-start(bf16[1,512,2048]{2,1,0:T(8,128)(2,1)} %param.40) | copy-start | bytes 6291460
  6.5 5.9 %copy-start.12 = (f32[16,64,16]{1,2,0:T(8,128)S(1)}, f32[16,64,16]{1,2,0:T(8,128)}, u32[]{:S(2)}) copy-start(f32[16,64,16]{1,2,0:T(8,128)} %param.27) | copy-start | bytes 196612
  6.5 5.9 %copy-start.11 = (f32[16,64,16]{1,2,0:T(8,128)S(1)}, f32[16,64,16]{1,2,0:T(8,128)}, u32[]{:S(2)}) copy-start(f32[16,64,16]{1,2,0:T(8,128)} %param.28) | copy-start | bytes 196612
  6.5 242.9 %all-gather.2.cloned.1.call-start = ((), (), s32[]{:S(2)}) async-start(), calls=%async_computation.3 | async-start | bytes 5242880 | tf_op jit(solution)/shard_map/all_gather | solution.py:171
  16.8 2.5 copy-start.23
  20.8 2.9 copy-start.1
  20.8 3.6 %copy-start.2 = (f32[256,16,64]{2,1,0:T(8,128)S(1)}, f32[256,16,64]{2,1,0:T(8,128)}, u32[]{:S(2)}) copy-start(f32[256,16,64]{2,1,0:T(8,128)} %copy.55) | copy-start | bytes 3145732
  26.0 2.0 copy-start.6
  26.0 2.7 copy-start.7
  26.0 3.3 copy-start.8
  29.4 13.7 %copy-start.16 = (f32[4,16,64]{2,1,0:T(8,128)}, f32[4,16,64]{2,1,0:T(8,128)S(1)}, u32[]{:S(2)}) copy-start(f32[4,16,64]{2,1,0:T(8,128)S(1)} %get-tuple-element.216) | copy-start | bytes 49156
  29.4 13.7 %copy-start.17 = (f32[4,16,64]{2,1,0:T(8,128)}, f32[4,16,64]{2,1,0:T(8,128)S(1)}, u32[]{:S(2)}) copy-start(f32[4,16,64]{2,1,0:T(8,128)S(1)} %get-tuple-element.217) | copy-start | bytes 49156
  29.4 3.1 copy-start.21
  50.0 25.6 %copy-start.13 = (bf16[256,256]{1,0:T(8,128)(2,1)S(1)}, bf16[256,256]{1,0:T(8,128)(2,1)}, u32[]{:S(2)}) copy-start(bf16[256,256]{1,0:T(8,128)(2,1)} %param.22) | copy-start | bytes 393220
  56.8 9.6 %copy-start.22 = (f32[1,16,64]{2,1,0:T(8,128)S(1)}, f32[1,16,64]{2,1,0:T(8,128)}, u32[]{:S(2)}) copy-start(f32[1,16,64]{2,1,0:T(8,128)} %get-tuple-element.249) | copy-start | bytes 12292
  62.0 22.6 %copy-start.18 = (f32[7,16,64]{2,1,0:T(8,128)S(1)}, f32[7,16,64]{2,1,0:T(8,128)}, u32[]{:S(2)}) copy-start(f32[7,16,64]{2,1,0:T(8,128)} %get-tuple-element.198) | copy-start | bytes 86020
  69.5 86.9 %slice-start = ((f32[15,16,64]{2,1,0:T(8,128)}), f32[1,16,64]{2,1,0:T(8,128)S(1)}, s32[]{:S(2)}) async-start(f32[15,16,64]{2,1,0:T(8,128)} %pad.268), calls=%async_computation.4 | async-start | bytes 16384 | tf_op jit(solution)/shard_map/slice | solution.py:143
  69.5 152.2 %copy-start.14 = (f32[15,16,64]{2,1,0:T(8,128)S(1)}, f32[15,16,64]{2,1,0:T(8,128)}, u32[]{:S(2)}) copy-start(f32[15,16,64]{2,1,0:T(8,128)} %pad.173) | copy-start | bytes 184324
  229.8 2.8 copy-start.19
  232.6 2.6 copy-start.9
  232.6 2.6 copy-start.29
  232.6 2.6 copy-start.30
  238.9 5.7 %copy-start.26 = (s32[64,2]{0,1:T(2,128)S(1)}, s32[64,2]{0,1:T(2,128)}, u32[]{:S(2)}) copy-start(s32[64,2]{0,1:T(2,128)} %param.36) | copy-start | bytes 1540
  239.0 10.5 %copy-start.15 = (bf16[64,2048]{1,0:T(8,128)(2,1)S(1)}, bf16[64,2048]{1,0:T(8,128)(2,1)}, u32[]{:S(2)}) copy-start(bf16[64,2048]{1,0:T(8,128)(2,1)} %param.34) | copy-start | bytes 786436
  239.0 10.5 %copy-start.25 = (f32[1024]{0:T(1024)S(1)}, f32[1024]{0:T(1024)}, u32[]{:S(2)}) copy-start(f32[1024]{0:T(1024)} %param.32) | copy-start | bytes 12292
  241.3 7.9 %all-to-all-start = ((bf16[4,64,256]{2,1,0:T(8,128)(2,1)}), bf16[4,64,256]{2,1,0:T(8,128)(2,1)S(1)}, u32[]{:S(2)}, u32[]{:S(2)}) async-start(bf16[4,64,256]{2,1,0:T(8,128)(2,1)} %all_to_all.16), calls=%async_computation | async-start | bytes 262144 | tf_op jit(solution)/shard_map/all_to_all | solution.py:165
  249.5 4.0 %copy-start.20 = (f32[2048]{0:T(1024)S(1)}, f32[2048]{0:T(1024)}, u32[]{:S(2)}) copy-start(f32[2048]{0:T(1024)} %param.35) | copy-start | bytes 24580
  255.0 32.2 %copy-start.28 = (bf16[1,2048,512]{2,1,0:T(8,128)(2,1)S(1)}, bf16[1,2048,512]{2,1,0:T(8,128)(2,1)}, u32[]{:S(2)}) copy-start(bf16[1,2048,512]{2,1,0:T(8,128)(2,1)} %param.38) | copy-start | bytes 6291460
  292.1 3.7 %copy-start.27 = (f32[64,2]{0,1:T(2,128)S(1)}, f32[64,2]{0,1:T(2,128)}, u32[]{:S(2)}) copy-start(f32[64,2]{0,1:T(2,128)} %param.37) | copy-start | bytes 1540
  292.1 29.2 %all-to-all-start.2 = ((bf16[8,32,2048]{2,1,0:T(8,128)(2,1)}), bf16[8,32,2048]{2,1,0:T(8,128)(2,1)S(1)}, u32[]{:S(2)}, u32[]{:S(2)}) async-start(bf16[8,32,2048]{2,1,0:T(8,128)(2,1)} %bitcast.122), calls=%async_computation.2 | async-start | bytes 2097152 | tf_op jit(solution)/shard_map/all_to_all | solution.py:198
  323.0 5.6 %copy-start.4 = (f32[64,2048]{1,0:T(8,128)S(1)}, f32[64,2048]{1,0:T(8,128)}, u32[]{:S(2)}) copy-start(f32[64,2048]{1,0:T(8,128)} %copy-done.3) | copy-start | bytes 1572868
  325.8 3.4 %copy-start.24 = (f32[2048]{0:T(1024)S(1)}, f32[2048]{0:T(1024)}, u32[]{:S(2)}) copy-start(f32[2048]{0:T(1024)} %param.41) | copy-start | bytes 24580
  (3 other events, 3.2 us)
Sparse Core Ops, SparseCore 0:
  8.9 37.1 all-gather.1
where the time goes:
time: 340 us; the launch traced here: 337 us
  blocking collectives  163 us (48%)
  local copies, waits for them, and re-layouts  66 us (19%)
  other arithmetic  41 us (12%)
  waiting for transfers between devices  28.7 us (8%)
  matrix products  17.5 us (5%)
  between operations  14.2 us (4%)
  starting transfers between devices  7.02 us (2%)
    all_gather x4, blocking collectives, prefix(): pieces = jax.tree.map(lambda part: lax.all_gather(part, axis), value)  131 us
    all_to_all x1, blocking collectives, local(): lax.all_to_all(outgoing, 'sp', split_axis=0, concat_axis=0, tiled=True)  31.2 us
    all_to_all x1, waiting for transfers between devices, local(): lax.all_to_all(produced.reshape(received.shape), 'sp', split_axis=0, conc...  25.4 us
    unnamed x69, local copies, waits for them, and re-layouts  18.5 us
    pad x22, local copies, waits for them, and re-layouts, local(): lax.associative_scan(chain_combine, (prefix_real[:, -1], prefix_imag[:, -...  16.8 us
    add x18, other arithmetic, local(): lax.associative_scan(chain_combine, (prefix_real[:, -1], prefix_imag[:, -...  8.31 us
    concatenate x12, other arithmetic, local(): lax.associative_scan(chain_combine, (prefix_real[:, -1], prefix_imag[:, -...  6.98 us
  transfers between devices with their start and end apart: 3, of which 2 were waited for; matrix products, arithmetic and copies ran while one was open for 29% of the time, Pallas kernels for 0%

commit v1 on v0

v1 whole, which is shorter than its diff:
```python
import functools

import jax
import jax.numpy as jnp
from jax import lax
from jax.experimental import pallas as pl
from jax.experimental.pallas import tpu as pltpu
from jax.sharding import PartitionSpec as P

PICKS = 2
deep_alpha = 2.0**0.25
lanes_of_chunks = 8
f32, bf16 = jnp.float32, jnp.bfloat16
VMEM = pltpu.VMEM


def power_of_two(count):
    return count & (count - 1) == 0


def swap(value, axis, distance):
    count = lax.axis_size(axis)
    return lax.ppermute(value, axis, [(i, i ^ distance) for i in range(count)])


def shift(value, axis, distance):
    count = lax.axis_size(axis)
    return lax.ppermute(value, axis, [(i, (i + distance) % count) for i in range(count)])


def pieces(value, count):
    out = []
    for _ in range(count):
        piece = value.astype(bf16)
        out.append(piece)
        value = value - piece.astype(f32)
    return out


def nt(left, right):
    return lax.dot_general(left, right, (((1,), (1,)), ((), ())), preferred_element_type=f32)


def nn(left, right):
    return lax.dot_general(left, right, (((1,), (0,)), ((), ())), preferred_element_type=f32)


def tn(left, right):
    return lax.dot_general(left, right, (((0,), (0,)), ((), ())), preferred_element_type=f32)


def reorder(count):
    steps = count // lanes_of_chunks
    row = lax.broadcasted_iota(jnp.int32, (count, count), 0)
    col = lax.broadcasted_iota(jnp.int32, (count, count), 1)
    source = (row % lanes_of_chunks) * steps + row // lanes_of_chunks
    return jnp.where(col == source, 1.0, 0.0).astype(bf16)


def lane_row(value):
    groups, width = value.shape
    per = 128 // width
    wide = jnp.concatenate([value] * per, axis=1)
    spot = lax.broadcasted_iota(jnp.int32, (1, 128), 1) // width
    parts = []
    for q in range(groups // per):
        row = wide[q * per : q * per + 1]
        for m in range(1, per):
            row = jnp.where(spot == m, wide[q * per + m : q * per + m + 1], row)
        parts.append(row)
    return jnp.concatenate(parts, axis=1)


def complex_times(ar, ai, br, bi):
    return ar * br - ai * bi, ar * bi + ai * br


def less_one(value):
    near = jnp.ones_like(value)
    for k in range(11, 1, -1):
        near = 1.0 + near * value / k
    return jnp.where(jnp.abs(value) < 0.5, near * value, jnp.exp(value) - 1.0)


def advance(block_r, block_i, shrink, keep_r, keep_i, drive_r, drive_i):
    turned_r, turned_i = complex_times(keep_r, keep_i, block_r, block_i)
    return shrink * turned_r + drive_r, shrink * turned_i + drive_i


def drive_kernel(
    u_ref, held_ref, real_ref, freq_ref, step_ref, in_r_ref, in_i_ref,
    drive_ref, shrink_ref, chunk_ref, total_ref,
):
    tokens, _ = u_ref.shape
    groups, states = real_ref.shape
    channels = in_r_ref.shape[1]
    width = groups * states
    steps = tokens // lanes_of_chunks
    log_step = step_ref[...]
    eye = lax.broadcasted_iota(jnp.int32, (groups, groups), 0) == lax.broadcasted_iota(
        jnp.int32, (groups, groups), 1
    )
    log_column = jnp.sum(jnp.where(eye, log_step, 0.0), axis=1, keepdims=True)
    stride = jnp.exp(log_column)
    decay_real, decay_freq = real_ref[...], freq_ref[...]
    growth = decay_real * stride
    turning = decay_freq * stride
    size = jnp.exp(growth)
    cosine, sine, half = jnp.cos(turning), jnp.sin(turning), jnp.sin(0.5 * turning)
    upper_real = less_one(growth) * cosine - 2.0 * half * half
    upper_imag = size * sine
    denominator = decay_real * decay_real + decay_freq * decay_freq
    factor_real = (upper_real * decay_real + upper_imag * decay_freq) / denominator
    factor_imag = (upper_imag * decay_real - upper_real * decay_freq) / denominator
    keep_r, keep_i = lane_row(size * cosine), lane_row(upper_imag)
    factor_r, factor_i = lane_row(factor_real), lane_row(factor_imag)

    order = reorder(tokens)
    moved = nn(order, u_ref[...])
    held = jnp.concatenate(pieces(jnp.exp(held_ref[...]), 3), axis=0)
    held = nt(held, order).astype(bf16)
    member = lax.broadcasted_iota(jnp.int32, (3 * groups, width), 0) % groups
    lane_group = lax.broadcasted_iota(jnp.int32, (3 * groups, width), 1) // states
    shrink_ref[...] = tn(held, jnp.where(member == lane_group, 1.0, 0.0).astype(bf16))

    block = 256 // states
    span, depth = block * states, block * channels
    row_group = lax.broadcasted_iota(jnp.int32, (span, depth), 0) // states
    col_group = lax.broadcasted_iota(jnp.int32, (span, depth), 1) // channels
    mask = row_group == col_group

    def spread(ref, at):
        wide = jnp.concatenate([ref[at : at + span, :]] * block, axis=1)
        return jnp.concatenate(pieces(jnp.where(mask, wide, 0.0), 3), axis=1)

    for n in range(width // span):
        left = moved[:, n * depth : (n + 1) * depth].astype(bf16)
        left = jnp.concatenate([left] * 3, axis=1)
        raw_r = nt(left, spread(in_r_ref, n * span))
        raw_i = nt(left, spread(in_i_ref, n * span))
        at = slice(n * span, (n + 1) * span)
        drive_r, drive_i = complex_times(factor_r[:, at], factor_i[:, at], raw_r, raw_i)
        drive_ref[0, :, at] = drive_r
        drive_ref[1, :, at] = drive_i

    zero = jnp.zeros((lanes_of_chunks, width), f32)

    def body(step, carry):
        state_r, state_i, gone = carry
        rows = pl.ds(pl.multiple_of(step * lanes_of_chunks, lanes_of_chunks), lanes_of_chunks)
        shrink = shrink_ref[rows, :]
        state_r, state_i = advance(
            state_r, state_i, shrink, keep_r, keep_i, drive_ref[0, rows, :], drive_ref[1, rows, :]
        )
        return state_r, state_i, gone * shrink

    state_r, state_i, gone = lax.fori_loop(0, steps, body, (zero, zero, zero + 1.0), unroll=2)
    power_r, power_i = jnp.ones_like(keep_r), jnp.zeros_like(keep_r)
    base_r, base_i, left_over = keep_r, keep_i, steps
    while left_over:
        if left_over & 1:
            power_r, power_i = complex_times(power_r, power_i, base_r, base_i)
        left_over >>= 1
        if left_over:
            base_r, base_i = complex_times(base_r, base_i, base_r, base_i)
    decay_r, decay_i = gone * power_r, gone * power_i
    chunk_ref[0], chunk_ref[1], chunk_ref[2], chunk_ref[3] = decay_r, decay_i, state_r, state_i
    chunk_ref[4] = jnp.broadcast_to(keep_r, zero.shape)
    chunk_ref[5] = jnp.broadcast_to(keep_i, zero.shape)
    all_r, all_i = decay_r[0:1], decay_i[0:1]
    end_r, end_i = state_r[0:1], state_i[0:1]
    for j in range(1, lanes_of_chunks):
        step_r, step_i = decay_r[j : j + 1], decay_i[j : j + 1]
        end_r, end_i = complex_times(step_r, step_i, end_r, end_i)
        end_r, end_i = end_r + state_r[j : j + 1], end_i + state_i[j : j + 1]
        all_r, all_i = complex_times(step_r, step_i, all_r, all_i)
    total_ref[0] = jnp.concatenate([all_r, all_i, end_r, end_i], axis=0)


def read_kernel(
    place_ref, u_ref, drive_ref, shrink_ref, chunk_ref, total_ref, out_r_ref, out_i_ref, skip_ref,
    mixed_ref, state_ref,
):
    tokens, depth = u_ref.shape
    width = shrink_ref.shape[1]
    members = total_ref.shape[0]
    steps = tokens // lanes_of_chunks
    place = place_ref[0]

    def earlier(member, carry):
        carry_r, carry_i = carry
        block = total_ref[member ^ place]
        next_r, next_i = complex_times(block[0:1], block[1:2], carry_r, carry_i)
        return next_r + block[2:3], next_i + block[3:4]

    start = jnp.zeros((1, width), f32)
    carry_r, carry_i = lax.fori_loop(0, place, earlier, (start, start))
    decay_r, decay_i, local_r, local_i = (chunk_ref[k] for k in range(4))
    keep_r, keep_i = chunk_ref[4], chunk_ref[5]
    rows_r, rows_i = [], []
    for j in range(lanes_of_chunks):
        rows_r.append(carry_r)
        rows_i.append(carry_i)
        one = slice(j, j + 1)
        carry_r, carry_i = complex_times(decay_r[one], decay_i[one], carry_r, carry_i)
        carry_r, carry_i = carry_r + local_r[one], carry_i + local_i[one]
    state = (jnp.concatenate(rows_r, axis=0), jnp.concatenate(rows_i, axis=0))

    def body(step, carry):
        rows = pl.ds(pl.multiple_of(step * lanes_of_chunks, lanes_of_chunks), lanes_of_chunks)
        state_r, state_i = advance(
            *carry, shrink_ref[rows, :], keep_r, keep_i, drive_ref[0, rows, :], drive_ref[1, rows, :]
        )
        state_ref[0, rows, :] = state_r
        state_ref[1, rows, :] = state_i
        return state_r, state_i

    lax.fori_loop(0, steps, body, state, unroll=2)
    groups, channels = skip_ref.shape
    states = width // groups
    block = 256 // states
    span, part = block * states, block * channels
    row_group = lax.broadcasted_iota(jnp.int32, (part, span), 0) // channels
    col_group = lax.broadcasted_iota(jnp.int32, (part, span), 1) // states
    mask = row_group == col_group
    outs = []
    for n in range(width // span):
        acc = None
        for k, ref in ((0, out_r_ref), (1, out_i_ref)):
            wide = jnp.concatenate([ref[n * part : (n + 1) * part, :]] * block, axis=1)
            wide = jnp.where(mask, wide, 0.0)
            wide = jnp.concatenate(pieces(-wide if k else wide, 2), axis=0)
            high, low = pieces(state_ref[k, :, n * span : (n + 1) * span], 2)
            first, second = nt(high, wide), nt(low, wide)
            term = first[:, :part] + first[:, part:] + second[:, :part]
            acc = term if acc is None else acc + term
        outs.append(acc)
    total = jnp.concatenate(outs, axis=1)
    order = reorder(tokens)
    total = total + lane_row(skip_ref[...]) * nn(order, u_ref[...])
    mixed = jax.nn.gelu(total).astype(bf16)
    back = tn(order, mixed).astype(bf16)
    rows = mixed_ref.shape[1]
    for k in range(mixed_ref.shape[0]):
        mixed_ref[k] = back[k * rows : (k + 1) * rows]


def whole(shape, dtype=f32):
    return jax.ShapeDtypeStruct(shape, dtype)


def layer_norm(values, scales):
    centered = values - jnp.mean(values, axis=-1, keepdims=True)
    variance = jnp.mean(centered * centered, axis=-1, keepdims=True)
    return centered * lax.rsqrt(variance + 1e-05) * scales


def gather_all(value, axis):
    count = lax.axis_size(axis)
    if not power_of_two(count):
        return None
    distance = 1
    while distance < count:
        value = jnp.concatenate([value, swap(value, axis, distance)], axis=0)
        distance *= 2
    return value


def exchange(blocks, axis, count):
    mine = lax.axis_index(axis)
    if count > 8:
        return lax.all_to_all(blocks, axis, split_axis=0, concat_axis=0, tiled=True)
    came = [lax.dynamic_index_in_dim(blocks, mine, 0, keepdims=True)]
    for distance in range(1, count):
        sent = lax.dynamic_index_in_dim(blocks, (mine + distance) % count, 0, keepdims=True)
        came.append(shift(sent, axis, distance))
    return came


def local(
    mixer_input, retention, decay_real, decay_freq, log_step, input_real, input_imag,
    readout_real, readout_imaginary, skip_weight, norm_gain, projection, residual, mix_gain,
    routes, route_weight, expert_gate, expert_up, expert_down, final_gain,
):
    token_count, depth = mixer_input.shape
    group_count, state_count = decay_real.shape
    channel_count = input_real.shape[2]
    width = group_count * state_count
    tp, sp = lax.axis_size("tp"), lax.axis_size("sp")
    tp_place, sp_place = lax.axis_index("tp"), lax.axis_index("sp")
    row_count = token_count // tp
    mix_width = depth * tp

    proj = projection[None]
    distance = tp // 2
    while distance:
        proj = jnp.concatenate([proj, swap(proj, "tp", distance)], axis=0)
        distance //= 2

    drive, shrink, chunk, total = pl.pallas_call(
        drive_kernel,
        out_shape=(
            whole((2, token_count, width)),
            whole((token_count, width)),
            whole((6, lanes_of_chunks, width)),
            whole((1, 4, width)),
        ),
        cost_estimate=pl.CostEstimate(flops=2 * 10**9, bytes_accessed=4 << 20, transcendentals=0),
        name="drive",
    )(
        mixer_input, retention, decay_real, decay_freq, log_step.reshape(1, group_count),
        input_real.reshape(width, channel_count), input_imag.reshape(width, channel_count),
    )
    totals = gather_all(total, "sp")
    mixed = pl.pallas_call(
        read_kernel,
        out_shape=whole((tp, row_count, depth), bf16),
        in_specs=[pl.BlockSpec(memory_space=pltpu.SMEM)] + [pl.BlockSpec(memory_space=VMEM)] * 8,
        scratch_shapes=[VMEM((2, token_count, width), f32)],
        cost_estimate=pl.CostEstimate(flops=2 * 10**9, bytes_accessed=4 << 20, transcendentals=0),
        name="readout",
    )(
        sp_place.reshape(1), mixer_input, drive, shrink, chunk, totals,
        readout_real.reshape(depth, state_count), readout_imaginary.reshape(depth, state_count),
        skip_weight,
    )

    order = [0]
    distance = tp // 2
    while distance:
        order = order + [k ^ distance for k in order]
        distance //= 2
    came = []
    for k in order:
        sent = lax.dynamic_index_in_dim(mixed, tp_place ^ k, 0, keepdims=False)
        came.append(sent if k == 0 else swap(sent, "tp", k))
    whole_rows = jnp.concatenate(came, axis=1)
    gain = norm_gain.reshape(tp, depth)
    gain = jnp.concatenate([lax.dynamic_index_in_dim(gain, tp_place ^ k, 0) for k in order], axis=1)
    whole_float = whole_rows.astype(f32)
    squares = jnp.sum(whole_float * whole_float, axis=1)
    scaled = (whole_float * gain).astype(bf16)
    summed = jnp.dot(scaled, proj.reshape(mix_width, -1), preferred_element_type=f32)
    mix = summed * lax.rsqrt(squares / mix_width + 1e-06)[:, None]
    hidden = layer_norm(deep_alpha * residual.astype(f32) + mix, mix_gain).astype(bf16)

    capacity = max(2, 2 * row_count * PICKS // sp)
    chosen = routes.reshape(-1)
    onehot = (chosen[:, None] == jnp.arange(sp, dtype=jnp.int32)[None, :]).astype(jnp.int32)
    slot_index = jnp.sum((jnp.cumsum(onehot, axis=0) - 1) * onehot, axis=1)
    target = chosen * capacity + slot_index
    source_row = jnp.full((sp * capacity,), row_count, jnp.int32)
    source_row = source_row.at[target].set(jnp.arange(row_count * PICKS, dtype=jnp.int32) // PICKS)
    padded = jnp.concatenate([hidden, jnp.zeros((1, hidden.shape[1]), hidden.dtype)], axis=0)
    outgoing = padded[source_row].reshape(sp, capacity, -1)
    received = lax.all_to_all(outgoing, "sp", split_axis=0, concat_axis=0, tiled=True)
    arrived = received.reshape(-1, received.shape[2])
    gate_act = jnp.dot(arrived, expert_gate[0], preferred_element_type=f32)
    up_act = jnp.dot(arrived, expert_up[0], preferred_element_type=f32)
    active = (jax.nn.silu(gate_act) * up_act).astype(bf16)
    produced = jnp.dot(active, expert_down[0], preferred_element_type=f32).astype(bf16)
    returned = lax.all_to_all(
        produced.reshape(received.shape), "sp", split_axis=0, concat_axis=0, tiled=True
    )
    gathered_rows = returned.reshape(sp * capacity, -1)[target].reshape(row_count, PICKS, -1)
    expert_mix = jnp.sum(route_weight[:, :, None] * gathered_rows.astype(f32), axis=1)
    layer_out = layer_norm(deep_alpha * hidden.astype(f32) + expert_mix, final_gain)
    return layer_out.astype(bf16)


def solution(mesh):
    in_specs = (
        P("sp", "tp"), P("tp", "sp"), P("tp", None), P("tp", None), P("tp"),
        P("tp", None, None), P("tp", None, None), P("tp", None, None), P("tp", None, None),
        P("tp", None), P(), P("tp", None), P(("sp", "tp"), None), P(),
        P(("sp", "tp"), None), P(("sp", "tp"), None),
        P("sp", None, None), P("sp", None, None), P("sp", None, None), P(),
    )
    out_specs = P(("sp", "tp"), None)
    return jax.shard_map(local, mesh=mesh, in_specs=in_specs, out_specs=out_specs, check_vma=False)
```

time: 340 us -> 133 us (0.39)
  blocking collectives: 163 us -> 31.2 us
  local copies, waits for them, and re-layouts: 66 us -> 13.6 us
  other arithmetic: 41 us -> 10.8 us
  waiting for transfers between devices: 28.7 us -> 45.6 us
  between operations: 14.2 us -> 0.29 us
  matrix products: 17.5 us -> 5.97 us
  Pallas kernels: 0 us -> 9.74 us
  starting transfers between devices: 7.02 us -> 15.4 us
    all_gather x4 -> x0, blocking collectives: 131 us -> none  [prefix(): pieces = jax.tree.map(lambda part: lax.all_gather(part, axis), value)]
    ppermute x0 -> x8, waiting for transfers between devices: none -> 20.3 us  [swap(): return lax.ppermute(value, axis, [(i, i ^ distance) for i in range(count)])]
    pad x22 -> x0, local copies, waits for them, and re-layouts: 16.8 us -> none  [local(): lax.associative_scan(chain_combine, (prefix_real[:, -1], prefix_imag[:, -...]
    add x29 -> x0, other arithmetic: 15.5 us -> none  [the longest x18 8.31 us: local(): lax.associative_scan(chain_combine, (prefix_real[:, -1], prefix_imag[:, -...]
    unnamed x69 -> x30, local copies, waits for them, and re-layouts: 18.5 us -> 5.57 us
    slice x14 -> x0, local copies, waits for them, and re-layouts: 11.9 us -> none  [the longest x9 4.52 us: local(): lax.associative_scan(chain_combine, (prefix_real[:, -1], prefix_imag[:, -...]
    dot_general x7 -> x3, matrix products: 17.5 us -> 5.97 us  [the longest x1 4.29 us: local(): jnp.dot(active, expert_down[0], preferred_element_type=f32).astype(bf16)]
    ppermute x0 -> x8, starting transfers between devices: none -> 11.5 us  [swap(): return lax.ppermute(value, axis, [(i, i ^ distance) for i in range(count)])]
  transfers between devices with their start and end apart: 3 -> 9, of which waited for: 2 -> 6; matrix products, arithmetic and copies ran while one was open for 29% -> 8% of each run, Pallas kernels for 0% -> 7%
where the time goes in v1:
time: 133 us
  waiting for transfers between devices  45.6 us (34%)
  blocking collectives  31.2 us (23%)
  starting transfers between devices  15.4 us (12%)
  local copies, waits for them, and re-layouts  13.6 us (10%)
  other arithmetic  10.8 us (8%)
  Pallas kernels  9.74 us (7%)
  matrix products  5.97 us (4%)
    all_to_all x1, blocking collectives, local(): lax.all_to_all(outgoing, 'sp', split_axis=0, concat_axis=0, tiled=True)  31.2 us
    all_to_all x1, waiting for transfers between devices, local(): lax.all_to_all(produced.reshape(received.shape), 'sp', split_axis=0, conc...  25.3 us
    ppermute x8, waiting for transfers between devices, swap(): return lax.ppermute(value, axis, [(i, i ^ distance) for i in range(count)])  20.3 us
    ppermute x8, starting transfers between devices, swap(): return lax.ppermute(value, axis, [(i, i ^ distance) for i in range(count)])  11.5 us
    unnamed x30, local copies, waits for them, and re-layouts  5.57 us
    pallas_call x1, Pallas kernels, local(): pl.pallas_call(drive_kernel, out_shape=(whole((2, token_count, width)), w...  5.39 us
    concatenate x2, other arithmetic, local(): proj = jnp.concatenate([proj, swap(proj, 'tp', distance)], axis=0)  4.82 us
    pallas_call x1, Pallas kernels, local(): pl.pallas_call(read_kernel, out_shape=whole((tp, row_count, depth), bf16)...  4.35 us
  transfers between devices with their start and end apart: 9, of which 6 were waited for; matrix products, arithmetic and copies ran while one was open for 8% of the time, Pallas kernels for 7%

profile of v1, /device:TPU:0, one launch (start us, length us, event | category | flops | bytes accessed | tf_op | source)
XLA Modules:
  0.0 132.5 jit_solution(13106138452666382444)
XLA Ops:
  0.0 3.0 %collective-permute-start.6 = (bf16[1,256,2048]{2,1,0:T(8,128)(2,1)}, bf16[1,256,2048]{2,1,0:T(8,128)(2,1)}, u32[]{:S(2)}, u32[]{:S(2)}) collective-permute-start(bf16[1,256,2048]{2,1,0:T(8,128)(2,1)} %bitcast.48), channel_id=1, source_target_pairs={{0,2},{1,3},{2,0},{3,1},{4,6},{5,7},{6,4},{7,5},{8,10},{9,11},{10,... | collective-permute-start | bytes 3145736 | tf_op jit(solution)/shard_map/ppermute | solution.py:23
  3.0 1.9 %copy.26 = f32[16,64,16]{2,1,0:T(8,128)} copy(f32[16,64,16]{1,2,0:T(8,128)} %param.25) | data formatting | bytes 131072 | tf_op args[5]
  4.9 1.9 %copy.27 = f32[16,64,16]{2,1,0:T(8,128)} copy(f32[16,64,16]{1,2,0:T(8,128)} %param.26) | data formatting | bytes 131072 | tf_op args[6]
  6.8 5.4 %drive.1 = (f32[2,256,1024]{2,1,0:T(8,128)}, f32[256,1024]{1,0:T(8,128)}, f32[6,8,1024]{2,1,0:T(8,128)}, f32[1,4,1024]{2,1,0:T(4,128)}) custom-call(bf16[256,256]{1,0:T(8,128)(2,1)} %u_ref.3, f32[16,256]{1,0:T(8,128)} %held_ref.1, f32[16,64]{1,0:T(8,128)} %real_ref.1, f32[16,64]{1,0:T(8,128)} %freq_ref.1, f32[1,16]{1,0:T(1,128)} %bitcast.59, ...), custom_call_target="tpu_custom_call" | custom-call | flops 2000000000 | bytes 4194304 | tf_op jit(solution)/shard_map/drive/pallas_call | solution.py:300
  12.2 1.5 %collective-permute-start = (f32[1,4,1024]{2,1,0:T(4,128)}, f32[1,4,1024]{2,1,0:T(4,128)S(1)}, u32[]{:S(2)}, u32[]{:S(2)}) collective-permute-start(f32[1,4,1024]{2,1,0:T(4,128)} %get-tuple-element.12), channel_id=1, source_target_pairs={{0,4},{4,0},{8,12},{12,8},{16,20},{20,16},{24,28},{28,24},{1,5},{5... | collective-permute-start | bytes 49160 | tf_op jit(solution)/shard_map/ppermute | solution.py:23
  14.2 12.3 %collective-permute-done.6 = bf16[1,256,2048]{2,1,0:T(8,128)(2,1)} collective-permute-done((bf16[1,256,2048]{2,1,0:T(8,128)(2,1)}, bf16[1,256,2048]{2,1,0:T(8,128)(2,1)}, u32[]{:S(2)}, u32[]{:S(2)}) %collective-permute-start.6) | collective-permute-done | bytes 1048608 | tf_op jit(solution)/shard_map/ppermute | solution.py:23
  26.4 2.7 %pad_maximum_fusion.1 = bf16[2,256,2048]{2,1,0:T(8,128)(2,1)} fusion(bf16[1,256,2048]{2,1,0:T(8,128)(2,1)} %collective-permute-done.6, bf16[1,256,2048]{2,1,0:T(8,128)(2,1)S(1)} %bitcast.49), kind=kLoop, calls=%fused_computation.7 | loop fusion | flops 1048576 | bytes 4194304 | tf_op jit(solution)/shard_map/concatenate | solution.py:297
  29.6 1.0 scatter_custom_fusion
  30.7 1.9 %collective-permute-start.1 = (f32[2,4,1024]{2,1,0:T(4,128)S(1)}, f32[2,4,1024]{2,1,0:T(4,128)S(1)}, u32[]{:S(2)}, u32[]{:S(2)}) collective-permute-start(f32[2,4,1024]{2,1,0:T(4,128)S(1)} %pad_maximum_fusion.5), channel_id=1, source_target_pairs={{0,8},{4,12},{8,0},{12,4},{16,24},{20,28},{24,16},{28,20},{1,9},{5... | collective-permute-start | bytes 98312 | tf_op jit(solution)/shard_map/ppermute | solution.py:23
  32.6 2.0 %collective-permute-done.1 = f32[2,4,1024]{2,1,0:T(4,128)S(1)} collective-permute-done((f32[2,4,1024]{2,1,0:T(4,128)S(1)}, f32[2,4,1024]{2,1,0:T(4,128)S(1)}, u32[]{:S(2)}, u32[]{:S(2)}) %collective-permute-start.1) | collective-permute-done | bytes 32800 | tf_op jit(solution)/shard_map/ppermute | solution.py:23
  34.7 2.9 %collective-permute-start.2 = (f32[4,4,1024]{2,1,0:T(4,128)S(1)}, f32[4,4,1024]{2,1,0:T(4,128)S(1)}, u32[]{:S(2)}, u32[]{:S(2)}) collective-permute-start(f32[4,4,1024]{2,1,0:T(4,128)S(1)} %pad_maximum_fusion.4), channel_id=1, source_target_pairs={{0,16},{4,20},{8,24},{12,28},{16,0},{20,4},{24,8},{28,12},{1,17},{... | collective-permute-start | bytes 196616 | tf_op jit(solution)/shard_map/ppermute | solution.py:23
  37.6 2.7 %collective-permute-done.2 = f32[4,4,1024]{2,1,0:T(4,128)S(1)} collective-permute-done((f32[4,4,1024]{2,1,0:T(4,128)S(1)}, f32[4,4,1024]{2,1,0:T(4,128)S(1)}, u32[]{:S(2)}, u32[]{:S(2)}) %collective-permute-start.2) | collective-permute-done | bytes 65568 | tf_op jit(solution)/shard_map/ppermute | solution.py:23
  40.2 0.7 pad_maximum_fusion.2.total_ref
  40.9 4.3 %readout.1 = bf16[4,64,256]{2,1,0:T(8,128)(2,1)} custom-call(s32[1]{0:T(128)} %bitcast.place_ref, bf16[256,256]{1,0:T(8,128)(2,1)} %u_ref.3, f32[2,256,1024]{2,1,0:T(8,128)} %get-tuple-element.9.drive_ref, f32[256,1024]{1,0:T(8,128)} %get-tuple-element.10.shrink_ref, f32[6,8,1024]{2,1,0:T(8,128)} %get-tuple-element.11.chunk_ref, ...), custom_call_target="tpu_custom_call" | custom-call | flops 2000000000 | bytes 4194304 | tf_op jit(solution)/shard_map/readout/pallas_call | solution.py:315
  45.3 0.8 dynamic-slice_bitcast_fusion.3
  46.2 1.6 %collective-permute-start.4 = (bf16[64,256]{1,0:T(8,128)(2,1)S(1)}, bf16[64,256]{1,0:T(8,128)(2,1)S(1)}, u32[]{:S(2)}, u32[]{:S(2)}) collective-permute-start(bf16[64,256]{1,0:T(8,128)(2,1)S(1)} %get-tuple-element.15), channel_id=1, source_target_pairs={{0,1},{1,0},{2,3},{3,2},{4,5},{5,4},{6,7},{7,6},{8,9},{9,8},{10,11... | collective-permute-start | bytes 98312 | tf_op jit(solution)/shard_map/ppermute | solution.py:23
  48.3 1.5 %collective-permute-done.5 = bf16[64,256]{1,0:T(8,128)(2,1)S(1)} collective-permute-done((bf16[64,256]{1,0:T(8,128)(2,1)S(1)}, bf16[64,256]{1,0:T(8,128)(2,1)S(1)}, u32[]{:S(2)}, u32[]{:S(2)}) %collective-permute-start.5) | collective-permute-done | bytes 32800 | tf_op jit(solution)/shard_map/ppermute | solution.py:23
  49.8 1.9 %collective-permute-done.3 = bf16[64,256]{1,0:T(8,128)(2,1)S(1)} collective-permute-done((bf16[64,256]{1,0:T(8,128)(2,1)S(1)}, bf16[64,256]{1,0:T(8,128)(2,1)S(1)}, u32[]{:S(2)}, u32[]{:S(2)}) %collective-permute-start.3) | collective-permute-done | bytes 32800 | tf_op jit(solution)/shard_map/ppermute | solution.py:23
  51.8 2.1 %pad_maximum_fusion = bf16[4,256,2048]{2,1,0:T(8,128)(2,1)S(1)} fusion(bf16[2,256,2048]{2,1,0:T(8,128)(2,1)} %collective-permute-done.7, bf16[1,256,2048]{2,1,0:T(8,128)(2,1)} %collective-permute-done.6, bf16[1,256,2048]{2,1,0:T(8,128)(2,1)S(1)} %bitcast.50), kind=kLoop, calls=%fused_computation.3 | loop fusion | flops 4194304 | bytes 8388608 | tf_op jit(solution)/shard_map/concatenate | solution.py:297
  54.0 1.0 fusion.31
  55.2 0.5 copy-done.1
  55.9 1.4 %gather_fusion = bf16[256,2048]{1,0:T(8,128)(2,1)S(1)} fusion(bf16[65,2048]{1,0:T(8,128)(2,1)S(1)} %concatenate.34, s32[1024]{0:T(1024)S(1)} %pad_clamp_fusion.1), kind=kCustom, calls=%fused_computation | custom fusion | bytes 2098176 | tf_op jit(solution)/shard_map/gather | solution.py:355
  57.3 31.2 %all_to_all.10 = bf16[8,32,2048]{2,1,0:T(8,128)(2,1)S(1)} all-to-all(bf16[8,32,2048]{2,1,0:T(8,128)(2,1)S(1)} %bitcast.47), channel_id=1, replica_groups=mesh['sp'=8,'tp'=4] {'sp'}, dimensions={0} | all-to-all | bytes 2097152 | tf_op jit(solution)/shard_map/all_to_all | solution.py:356
  88.5 1.0 copy-done.4
  89.4 0.7 fusion.4
  90.1 4.3 %convolution_convert_fusion = bf16[256,2048]{1,0:T(8,128)(2,1)} fusion(bf16[1,512,2048]{2,1,0:T(8,128)(2,1)S(1)} %copy-done, bf16[256,2048]{1,0:T(8,128)(2,1)} %bitcast.53, bf16[1,2048,512]{2,1,0:T(8,128)(2,1)} %param.37, f32[256,512]{1,0:T(8,128)S(1)} %fusion.4), kind=kOutput, calls=%fused_computation.4 | convolution fusion | flops 1075052544 | bytes 6815744 | tf_op jit(solution)/shard_map/dot_general | solution.py:361
  94.4 3.9 %all-to-all-start.1 = ((bf16[8,32,2048]{2,1,0:T(8,128)(2,1)}), bf16[8,32,2048]{2,1,0:T(8,128)(2,1)S(1)}, u32[]{:S(2)}, u32[]{:S(2)}) async-start(bf16[8,32,2048]{2,1,0:T(8,128)(2,1)} %bitcast.51), calls=%async_computation.1 | async-start | bytes 2097152 | tf_op jit(solution)/shard_map/all_to_all | solution.py:362
  98.4 25.3 %all-to-all-done.1 = bf16[8,32,2048]{2,1,0:T(8,128)(2,1)S(1)} async-done(((bf16[8,32,2048]{2,1,0:T(8,128)(2,1)}), bf16[8,32,2048]{2,1,0:T(8,128)(2,1)S(1)}, u32[]{:S(2)}, u32[]{:S(2)}) %all-to-all-start.1) | async-done | bytes 1048608 | tf_op jit(solution)/shard_map/all_to_all | solution.py:362
  123.7 1.7 %gather_fusion.1 = bf16[128,2048]{1,0:T(8,128)(2,1)} fusion(bf16[256,2048]{1,0:T(8,128)(2,1)S(1)} %bitcast.45, s32[1024]{0:T(1024)S(1)} %pad_clamp_fusion), kind=kCustom, calls=%fused_computation.1 | custom fusion | bytes 1049088 | tf_op jit(solution)/shard_map/gather | solution.py:365
  125.4 2.7 %reshape.113 = f32[64,2,2048]{2,1,0:T(2,128)} reshape(bf16[128,2048]{1,0:T(8,128)(2,1)} %gather_fusion.1) | data formatting | bytes 1572864 | tf_op jit(solution)/shard_map/convert_element_type | solution.py:366
  128.2 2.8 %multiply_reduce_fusion = f32[64,2048]{1,0:T(8,128)S(1)} fusion(f32[64,2,2048]{2,1,0:T(2,128)} %reshape.113, f32[64,2]{1,0:T(8,128)S(1)} %copy.28), kind=kLoop, calls=%fused_computation.15 | loop fusion | flops 393216 | bytes 1573376 | tf_op jit(solution)/shard_map/reduce_sum | solution.py:366
  131.5 1.0 multiply_convert_fusion
  (60 shorter events, 2.9 us)
Async XLA Ops:
  0.0 90.1 %copy-start = (bf16[1,512,2048]{2,1,0:T(8,128)(2,1)S(1)}, bf16[1,512,2048]{2,1,0:T(8,128)(2,1)}, u32[]{:S(2)}) copy-start(bf16[1,512,2048]{2,1,0:T(8,128)(2,1)} %param.38) | copy-start | bytes 6291460
  0.0 26.4 %collective-permute-start.6 = (bf16[1,256,2048]{2,1,0:T(8,128)(2,1)}, bf16[1,256,2048]{2,1,0:T(8,128)(2,1)}, u32[]{:S(2)}, u32[]{:S(2)}) collective-permute-start(bf16[1,256,2048]{2,1,0:T(8,128)(2,1)} %bitcast.48), channel_id=1, source_target_pairs={{0,2},{1,3},{2,0},{3,1},{4,6},{5,7},{6,4},{7,5},{8,10},{9,11},{10,... | collective-permute-start | bytes 3145736 | tf_op jit(solution)/shard_map/ppermute | solution.py:23
  6.8 6.9 %copy-start.9 = (s32[64,2]{0,1:T(2,128)S(1)}, s32[64,2]{0,1:T(2,128)}, u32[]{:S(2)}) copy-start(s32[64,2]{0,1:T(2,128)} %param.34) | copy-start | bytes 1540
  6.8 19.7 %copy-start.3 = (bf16[256,2048]{1,0:T(8,128)(2,1)S(1)}, bf16[256,2048]{1,0:T(8,128)(2,1)}, u32[]{:S(2)}) copy-start(bf16[256,2048]{1,0:T(8,128)(2,1)} %param.31) | copy-start | bytes 3145732
  12.2 18.5 %collective-permute-start = (f32[1,4,1024]{2,1,0:T(4,128)}, f32[1,4,1024]{2,1,0:T(4,128)S(1)}, u32[]{:S(2)}, u32[]{:S(2)}) collective-permute-start(f32[1,4,1024]{2,1,0:T(4,128)} %get-tuple-element.12), channel_id=1, source_target_pairs={{0,4},{4,0},{8,12},{12,8},{16,20},{20,16},{24,28},{28,24},{1,5},{5... | collective-permute-start | bytes 49160 | tf_op jit(solution)/shard_map/ppermute | solution.py:23
  14.2 16.5 %copy-start.6 = (f32[1,4,1024]{2,1,0:T(4,128)S(1)}, f32[1,4,1024]{2,1,0:T(4,128)}, u32[]{:S(2)}) copy-start(f32[1,4,1024]{2,1,0:T(4,128)} %get-tuple-element.12) | copy-start | bytes 49156
  14.2 18.4 %copy-start.10 = (f32[1024]{0:T(1024)S(1)}, f32[1024]{0:T(1024)}, u32[]{:S(2)}) copy-start(f32[1024]{0:T(1024)} %param.30) | copy-start | bytes 12292
  29.2 22.7 %collective-permute-start.7 = (bf16[2,256,2048]{2,1,0:T(8,128)(2,1)}, bf16[2,256,2048]{2,1,0:T(8,128)(2,1)}, u32[]{:S(2)}, u32[]{:S(2)}) collective-permute-start(bf16[2,256,2048]{2,1,0:T(8,128)(2,1)} %pad_maximum_fusion.1), channel_id=1, source_target_pairs={{0,1},{1,0},{2,3},{3,2},{4,5},{5,4},{6,7},{7,6},{8,9},{9,8},{10,11... | collective-permute-start | bytes 6291464 | tf_op jit(solution)/shard_map/ppermute | solution.py:23
  30.7 4.0 %collective-permute-start.1 = (f32[2,4,1024]{2,1,0:T(4,128)S(1)}, f32[2,4,1024]{2,1,0:T(4,128)S(1)}, u32[]{:S(2)}, u32[]{:S(2)}) collective-permute-start(f32[2,4,1024]{2,1,0:T(4,128)S(1)} %pad_maximum_fusion.5), channel_id=1, source_target_pairs={{0,8},{4,12},{8,0},{12,4},{16,24},{20,28},{24,16},{28,20},{1,9},{5... | collective-permute-start | bytes 98312 | tf_op jit(solution)/shard_map/ppermute | solution.py:23
  34.7 5.6 %collective-permute-start.2 = (f32[4,4,1024]{2,1,0:T(4,128)S(1)}, f32[4,4,1024]{2,1,0:T(4,128)S(1)}, u32[]{:S(2)}, u32[]{:S(2)}) collective-permute-start(f32[4,4,1024]{2,1,0:T(4,128)S(1)} %pad_maximum_fusion.4), channel_id=1, source_target_pairs={{0,16},{4,20},{8,24},{12,28},{16,0},{20,4},{24,8},{28,12},{1,17},{... | collective-permute-start | bytes 196616 | tf_op jit(solution)/shard_map/ppermute | solution.py:23
  46.1 3.7 %collective-permute-start.5 = (bf16[64,256]{1,0:T(8,128)(2,1)S(1)}, bf16[64,256]{1,0:T(8,128)(2,1)S(1)}, u32[]{:S(2)}, u32[]{:S(2)}) collective-permute-start(bf16[64,256]{1,0:T(8,128)(2,1)S(1)} %get-tuple-element.14), channel_id=1, source_target_pairs={{0,3},{1,2},{2,1},{3,0},{4,7},{5,6},{6,5},{7,4},{8,11},{9,10},{10,... | collective-permute-start | bytes 98312 | tf_op jit(solution)/shard_map/ppermute | solution.py:23
  46.2 3.6 %collective-permute-start.4 = (bf16[64,256]{1,0:T(8,128)(2,1)S(1)}, bf16[64,256]{1,0:T(8,128)(2,1)S(1)}, u32[]{:S(2)}, u32[]{:S(2)}) collective-permute-start(bf16[64,256]{1,0:T(8,128)(2,1)S(1)} %get-tuple-element.15), channel_id=1, source_target_pairs={{0,1},{1,0},{2,3},{3,2},{4,5},{5,4},{6,7},{7,6},{8,9},{9,8},{10,11... | collective-permute-start | bytes 98312 | tf_op jit(solution)/shard_map/ppermute | solution.py:23
  47.8 3.9 %collective-permute-start.3 = (bf16[64,256]{1,0:T(8,128)(2,1)S(1)}, bf16[64,256]{1,0:T(8,128)(2,1)S(1)}, u32[]{:S(2)}, u32[]{:S(2)}) collective-permute-start(bf16[64,256]{1,0:T(8,128)(2,1)S(1)} %get-tuple-element.16), channel_id=1, source_target_pairs={{0,2},{1,3},{2,0},{3,1},{4,6},{5,7},{6,4},{7,5},{8,10},{9,11},{10,... | collective-permute-start | bytes 98312 | tf_op jit(solution)/shard_map/ppermute | solution.py:23
  51.8 2.1 %copy-start.5 = (bf16[64,2048]{1,0:T(8,128)(2,1)S(1)}, bf16[64,2048]{1,0:T(8,128)(2,1)}, u32[]{:S(2)}) copy-start(bf16[64,2048]{1,0:T(8,128)(2,1)} %param.32) | copy-start | bytes 786436
  53.9 1.8 %copy-start.7 = (f32[2048]{0:T(1024)S(1)}, f32[2048]{0:T(1024)}, u32[]{:S(2)}) copy-start(f32[2048]{0:T(1024)} %param.33) | copy-start | bytes 24580
  55.0 0.8 copy-start.1
  57.3 32.1 %copy-start.12 = (bf16[1,2048,512]{2,1,0:T(8,128)(2,1)S(1)}, bf16[1,2048,512]{2,1,0:T(8,128)(2,1)}, u32[]{:S(2)}) copy-start(bf16[1,2048,512]{2,1,0:T(8,128)(2,1)} %param.36) | copy-start | bytes 6291460
  88.5 1.0 copy-start.4
  94.4 3.9 %copy-start.11 = (f32[64,2]{0,1:T(2,128)S(1)}, f32[64,2]{0,1:T(2,128)}, u32[]{:S(2)}) copy-start(f32[64,2]{0,1:T(2,128)} %param.35) | copy-start | bytes 1540
  94.4 29.2 %all-to-all-start.1 = ((bf16[8,32,2048]{2,1,0:T(8,128)(2,1)}), bf16[8,32,2048]{2,1,0:T(8,128)(2,1)S(1)}, u32[]{:S(2)}, u32[]{:S(2)}) async-start(bf16[8,32,2048]{2,1,0:T(8,128)(2,1)} %bitcast.51), calls=%async_computation.1 | async-start | bytes 2097152 | tf_op jit(solution)/shard_map/all_to_all | solution.py:362
  125.4 5.5 %copy-start.2 = (f32[64,2048]{1,0:T(8,128)S(1)}, f32[64,2048]{1,0:T(8,128)}, u32[]{:S(2)}) copy-start(f32[64,2048]{1,0:T(8,128)} %copy-done.1) | copy-start | bytes 1572868
  128.1 3.4 %copy-start.8 = (f32[2048]{0:T(1024)S(1)}, f32[2048]{0:T(1024)}, u32[]{:S(2)}) copy-start(f32[2048]{0:T(1024)} %param.39) | copy-start | bytes 24580

commit v2 on v1

--- a/solution.py
+++ b/solution.py
@@ -93,7 +93,7 @@
 ):
     tokens, _ = u_ref.shape
     groups, states = real_ref.shape
-    channels = in_r_ref.shape[1]
+    channels = in_r_ref.shape[0] // groups
     width = groups * states
     steps = tokens // lanes_of_chunks
     log_step = step_ref[...]
@@ -125,19 +125,19 @@
 
     block = 256 // states
     span, depth = block * states, block * channels
-    row_group = lax.broadcasted_iota(jnp.int32, (span, depth), 0) // states
-    col_group = lax.broadcasted_iota(jnp.int32, (span, depth), 1) // channels
+    row_group = lax.broadcasted_iota(jnp.int32, (depth, span), 0) // channels
+    col_group = lax.broadcasted_iota(jnp.int32, (depth, span), 1) // states
     mask = row_group == col_group
 
     def spread(ref, at):
-        wide = jnp.concatenate([ref[at : at + span, :]] * block, axis=1)
-        return jnp.concatenate(pieces(jnp.where(mask, wide, 0.0), 3), axis=1)
+        wide = jnp.concatenate([ref[at : at + depth, :]] * block, axis=1)
+        return jnp.concatenate(pieces(jnp.where(mask, wide, 0.0), 3), axis=0)
 
     for n in range(width // span):
         left = moved[:, n * depth : (n + 1) * depth].astype(bf16)
         left = jnp.concatenate([left] * 3, axis=1)
-        raw_r = nt(left, spread(in_r_ref, n * span))
-        raw_i = nt(left, spread(in_i_ref, n * span))
+        raw_r = nn(left, spread(in_r_ref, n * depth))
+        raw_i = nn(left, spread(in_i_ref, n * depth))
         at = slice(n * span, (n + 1) * span)
         drive_r, drive_i = complex_times(factor_r[:, at], factor_i[:, at], raw_r, raw_i)
         drive_ref[0, :, at] = drive_r
@@ -178,12 +178,15 @@
 
 
 def read_kernel(
-    place_ref, u_ref, drive_ref, shrink_ref, chunk_ref, total_ref, out_r_ref, out_i_ref, skip_ref,
-    mixed_ref, state_ref,
+    place_ref, u_ref, drive_ref, shrink_ref, chunk_ref, near_ref, far_ref, out_r_ref, out_i_ref,
+    skip_ref, *rest,
 ):
+    *mixed_refs, state_ref, total_ref, back_ref = rest
     tokens, depth = u_ref.shape
     width = shrink_ref.shape[1]
-    members = total_ref.shape[0]
+    half = near_ref.shape[0]
+    total_ref[:half] = near_ref[...]
+    total_ref[half:] = far_ref[...]
     steps = tokens // lanes_of_chunks
     place = place_ref[0]
 
@@ -239,10 +242,19 @@
     order = reorder(tokens)
     total = total + lane_row(skip_ref[...]) * nn(order, u_ref[...])
     mixed = jax.nn.gelu(total).astype(bf16)
-    back = tn(order, mixed).astype(bf16)
-    rows = mixed_ref.shape[1]
-    for k in range(mixed_ref.shape[0]):
-        mixed_ref[k] = back[k * rows : (k + 1) * rows]
+    back_ref[...] = tn(order, mixed).astype(bf16)
+    rows = mixed_refs[0].shape[0]
+    for ref, k in zip(mixed_refs, doubling(len(mixed_refs))):
+        at = pl.multiple_of((place_ref[1] ^ k) * rows, rows)
+        ref[...] = back_ref[pl.ds(at, rows), :]
+
+
+def doubling(count):
+    order, distance = [0], count // 2
+    while distance:
+        order = order + [k ^ distance for k in order]
+        distance //= 2
+    return order
 
 
 def whole(shape, dtype=f32):
@@ -255,26 +267,118 @@
     return centered * lax.rsqrt(variance + 1e-05) * scales
 
 
-def gather_all(value, axis):
-    count = lax.axis_size(axis)
-    if not power_of_two(count):
-        return None
-    distance = 1
-    while distance < count:
-        value = jnp.concatenate([value, swap(value, axis, distance)], axis=0)
-        distance *= 2
-    return value
-
-
-def exchange(blocks, axis, count):
-    mine = lax.axis_index(axis)
-    if count > 8:
-        return lax.all_to_all(blocks, axis, split_axis=0, concat_axis=0, tiled=True)
-    came = [lax.dynamic_index_in_dim(blocks, mine, 0, keepdims=True)]
-    for distance in range(1, count):
-        sent = lax.dynamic_index_in_dim(blocks, (mine + distance) % count, 0, keepdims=True)
-        came.append(shift(sent, axis, distance))
-    return came
+def route_kernel(capacity, relative, place_ref, routes_ref, weight_ref, pick_ref, join_ref):
+    rows, picks = routes_ref.shape
+    slots = pick_ref.shape[0]
+    experts = slots // capacity
+    routes = routes_ref[...]
+    if relative:
+        routes = routes ^ place_ref[0]
+    iota = functools.partial(lax.broadcasted_iota, jnp.int32)
+    eye = jnp.where(iota((rows, rows), 0) == iota((rows, rows), 1), 1.0, 0.0).astype(bf16)
+    before = jnp.where(iota((rows, rows), 0) < iota((rows, rows), 1), 1.0, 0.0).astype(bf16)
+    chosen = tn(routes.astype(f32).astype(bf16), eye)
+    weight = sum(tn(piece, eye) for piece in pieces(weight_ref[...], 3))
+    expert = iota((experts, rows), 0).astype(f32)
+    named, share = 0.0, 0.0
+    for k in range(picks):
+        hit = expert == chosen[k : k + 1]
+        named = named + jnp.where(hit, 1.0, 0.0)
+        share = share + jnp.where(hit, weight[k : k + 1], 0.0)
+    slot = nn(named.astype(bf16), before)
+    owner = jnp.where(iota((slots, experts), 0) // capacity == iota((slots, experts), 1), 1.0, 0.0)
+    owner = owner.astype(bf16)
+    place = (iota((slots, rows), 0) % capacity).astype(f32)
+    picked = (nn(owner, slot.astype(bf16)) == place) & (nn(owner, named.astype(bf16)) > 0.5)
+    pick_ref[...] = jnp.where(picked, 1.0, 0.0).astype(bf16)
+    shares = sum(nn(owner, piece) for piece in pieces(share, 3))
+    join_ref[...] = jnp.concatenate(pieces(jnp.where(picked, shares, 0.0), 3), axis=1)
+
+
+def hidden_kernel(
+    count, place_ref, gain_ref, residual_ref, mix_gain_ref, pick_ref, *rest
+):
+    parts, projs, rest = rest[:count], rest[count : 2 * count], rest[2 * count :]
+    hidden_ref, *out_refs, proj_ref, sems = rest
+    depth = parts[0].shape[1]
+    copies = []
+    for k in range(count):
+        copy = pltpu.make_async_copy(projs[k], proj_ref.at[k], sems.at[k])
+        copy.start()
+        copies.append(copy)
+    squares, total = 0.0, 0.0
+    for k, distance in enumerate(doubling(count)):
+        part = parts[k][...].astype(f32)
+        squares = squares + jnp.sum(part * part, axis=1, keepdims=True)
+        scaled = (part * gain_ref[pl.ds(place_ref[1] ^ distance, 1), :]).astype(bf16)
+        copies[k].wait()
+        total = total + nn(scaled, proj_ref[k])
+    mix = total * lax.rsqrt(squares / (depth * count) + 1e-06)
+    hidden = layer_norm(deep_alpha * residual_ref[...].astype(f32) + mix, mix_gain_ref[...])
+    hidden = hidden.astype(bf16)
+    hidden_ref[...] = hidden
+    start = 0
+    for ref in out_refs:
+        size = ref.shape[0]
+        ref[...] = nn(pick_ref[start : start + size, :], hidden).astype(bf16)
+        start += size
+
+
+def expert_kernel(count, gate_ref, up_ref, down_ref, *rest):
+    in_refs, out_refs, (rows_ref, sum_ref) = rest[:count], rest[count : 2 * count], rest[2 * count :]
+    size = in_refs[0].shape[0]
+    step = pl.program_id(0)
+
+    @pl.when(step == 0)
+    def _():
+        for k, ref in enumerate(in_refs):
+            rows_ref[k * size : (k + 1) * size, :] = ref[...]
+        sum_ref[...] = jnp.zeros_like(sum_ref)
+
+    rows = rows_ref[...]
+    active = (jax.nn.silu(nn(rows, gate_ref[0])) * nn(rows, up_ref[0])).astype(bf16)
+    sum_ref[...] += nn(active, down_ref[0])
+
+    @pl.when(step == pl.num_programs(0) - 1)
+    def _():
+        for k, ref in enumerate(out_refs):
+            ref[...] = sum_ref[k * size : (k + 1) * size, :].astype(bf16)
+
+
+def experts(blocks, gate, up, down):
+    _, width, inner = gate.shape
+    size = blocks[0].shape[0]
+    count = len(blocks)
+    tile = min(inner, 256)
+    full = pl.BlockSpec((size, width), lambda h: (0, 0))
+    return pl.pallas_call(
+        functools.partial(expert_kernel, count),
+        grid=(inner // tile,),
+        out_shape=[whole((size, width), bf16)] * count,
+        in_specs=[
+            pl.BlockSpec((1, width, tile), lambda h: (0, 0, h)),
+            pl.BlockSpec((1, width, tile), lambda h: (0, 0, h)),
+            pl.BlockSpec((1, tile, width), lambda h: (0, h, 0)),
+        ]
+        + [full] * count,
+        out_specs=[full] * count,
+        scratch_shapes=[VMEM((count * size, width), bf16), VMEM((count * size, width), f32)],
+        cost_estimate=pl.CostEstimate(flops=10**9, bytes_accessed=6 << 20, transcendentals=0),
+        name="experts",
+    )(gate, up, down, *blocks)
+
+
+def final_kernel(hidden_ref, join_ref, gain_ref, *rest):
+    *in_refs, out_ref, rows_ref = rest
+    rows = hidden_ref.shape[0]
+    start = 0
+    for ref in in_refs:
+        rows_ref[start : start + ref.shape[0], :] = ref[...]
+        start += ref.shape[0]
+    parts = tn(join_ref[...], rows_ref[...])
+    expert_mix = parts[:rows] + parts[rows : 2 * rows] + parts[2 * rows :]
+    values = deep_alpha * hidden_ref[...].astype(f32) + expert_mix
+    out_ref[...] = layer_norm(values, gain_ref[...]).astype(bf16)
 
 
 def local(
@@ -284,18 +388,17 @@
 ):
     token_count, depth = mixer_input.shape
     group_count, state_count = decay_real.shape
-    channel_count = input_real.shape[2]
     width = group_count * state_count
     tp, sp = lax.axis_size("tp"), lax.axis_size("sp")
-    tp_place, sp_place = lax.axis_index("tp"), lax.axis_index("sp")
-    row_count = token_count // tp
-    mix_width = depth * tp
-
-    proj = projection[None]
+    place = jnp.stack([lax.axis_index("sp"), lax.axis_index("tp")])
+    row_count, model = residual.shape
+    smem, vmem = pl.BlockSpec(memory_space=pltpu.SMEM), pl.BlockSpec(memory_space=VMEM)
+    hbm = pl.BlockSpec(memory_space=pl.ANY)
+    cost = functools.partial(pl.CostEstimate, transcendentals=0)
+
+    proj = {0: projection}
     distance = tp // 2
-    while distance:
-        proj = jnp.concatenate([proj, swap(proj, "tp", distance)], axis=0)
-        distance //= 2
+    proj[distance] = swap(projection, "tp", distance)
 
     drive, shrink, chunk, total = pl.pallas_call(
         drive_kernel,
@@ -305,67 +408,107 @@
             whole((6, lanes_of_chunks, width)),
             whole((1, 4, width)),
         ),
-        cost_estimate=pl.CostEstimate(flops=2 * 10**9, bytes_accessed=4 << 20, transcendentals=0),
+        cost_estimate=cost(flops=2 * 10**9, bytes_accessed=4 << 20),
         name="drive",
     )(
         mixer_input, retention, decay_real, decay_freq, log_step.reshape(1, group_count),
-        input_real.reshape(width, channel_count), input_imag.reshape(width, channel_count),
+        input_real.transpose(0, 2, 1).reshape(depth, state_count),
+        input_imag.transpose(0, 2, 1).reshape(depth, state_count),
     )
-    totals = gather_all(total, "sp")
+
+    near, far, distance = total, None, 1
+    while distance < sp:
+        if far is not None:
+            near = jnp.concatenate([near, far], axis=0)
+        far = swap(near, "sp", distance)
+        distance *= 2
+
+    capacity = max(2, 2 * row_count * PICKS // sp)
+    relative = sp <= 8
+    late_routes, _ = lax.optimization_barrier((routes, total))
+    pick, join = pl.pallas_call(
+        functools.partial(route_kernel, capacity, relative),
+        out_shape=(
+            whole((sp * capacity, row_count), bf16),
+            whole((sp * capacity, 3 * row_count), bf16),
+        ),
+        in_specs=[smem, vmem, vmem],
+        cost_estimate=cost(flops=10**8, bytes_accessed=1 << 17),
+        name="route",
+    )(place, late_routes, route_weight)
+
     mixed = pl.pallas_call(
         read_kernel,
-        out_shape=whole((tp, row_count, depth), bf16),
-        in_specs=[pl.BlockSpec(memory_space=pltpu.SMEM)] + [pl.BlockSpec(memory_space=VMEM)] * 8,
-        scratch_shapes=[VMEM((2, token_count, width), f32)],
-        cost_estimate=pl.CostEstimate(flops=2 * 10**9, bytes_accessed=4 << 20, transcendentals=0),
+        out_shape=[whole((row_count, depth), bf16)] * tp,
+        in_specs=[smem] + [vmem] * 9,
+        scratch_shapes=[
+            VMEM((2, token_count, width), f32),
+            VMEM((sp, 4, width), f32),
+            VMEM((token_count, depth), bf16),
+        ],
+        cost_estimate=cost(flops=2 * 10**9, bytes_accessed=4 << 20),
         name="readout",
     )(
-        sp_place.reshape(1), mixer_input, drive, shrink, chunk, totals,
+        place, mixer_input, drive, shrink, chunk, near, far,
         readout_real.reshape(depth, state_count), readout_imaginary.reshape(depth, state_count),
         skip_weight,
     )
 
-    order = [0]
+    parts = [part if k == 0 else swap(part, "tp", k) for part, k in zip(mixed, doubling(tp))]
     distance = tp // 2
+    held = [projection, lax.optimization_barrier((proj[distance], mixed[0]))[0]]
+    held[0] = lax.optimization_barrier((projection, mixed[0]))[0]
+    proj[distance] = held[1]
+    sources = dict(proj)
+    sources[0] = held[0]
+    distance //= 2
     while distance:
-        order = order + [k ^ distance for k in order]
+        for k in list(sources):
+            sources[k ^ distance] = swap(sources[k], "tp", distance)
         distance //= 2
-    came = []
-    for k in order:
-        sent = lax.dynamic_index_in_dim(mixed, tp_place ^ k, 0, keepdims=False)
-        came.append(sent if k == 0 else swap(sent, "tp", k))
-    whole_rows = jnp.concatenate(came, axis=1)
-    gain = norm_gain.reshape(tp, depth)
-    gain = jnp.concatenate([lax.dynamic_index_in_dim(gain, tp_place ^ k, 0) for k in order], axis=1)
-    whole_float = whole_rows.astype(f32)
-    squares = jnp.sum(whole_float * whole_float, axis=1)
-    scaled = (whole_float * gain).astype(bf16)
-    summed = jnp.dot(scaled, proj.reshape(mix_width, -1), preferred_element_type=f32)
-    mix = summed * lax.rsqrt(squares / mix_width + 1e-06)[:, None]
-    hidden = layer_norm(deep_alpha * residual.astype(f32) + mix, mix_gain).astype(bf16)
-
-    capacity = max(2, 2 * row_count * PICKS // sp)
-    chosen = routes.reshape(-1)
-    onehot = (chosen[:, None] == jnp.arange(sp, dtype=jnp.int32)[None, :]).astype(jnp.int32)
-    slot_index = jnp.sum((jnp.cumsum(onehot, axis=0) - 1) * onehot, axis=1)
-    target = chosen * capacity + slot_index
-    source_row = jnp.full((sp * capacity,), row_count, jnp.int32)
-    source_row = source_row.at[target].set(jnp.arange(row_count * PICKS, dtype=jnp.int32) // PICKS)
-    padded = jnp.concatenate([hidden, jnp.zeros((1, hidden.shape[1]), hidden.dtype)], axis=0)
-    outgoing = padded[source_row].reshape(sp, capacity, -1)
-    received = lax.all_to_all(outgoing, "sp", split_axis=0, concat_axis=0, tiled=True)
-    arrived = received.reshape(-1, received.shape[2])
-    gate_act = jnp.dot(arrived, expert_gate[0], preferred_element_type=f32)
-    up_act = jnp.dot(arrived, expert_up[0], preferred_element_type=f32)
-    active = (jax.nn.silu(gate_act) * up_act).astype(bf16)
-    produced = jnp.dot(active, expert_down[0], preferred_element_type=f32).astype(bf16)
-    returned = lax.all_to_all(
-        produced.reshape(received.shape), "sp", split_axis=0, concat_axis=0, tiled=True
+    sources[0] = projection
+
+    blocks = sp if relative else 1
+    hidden, *outgoing = pl.pallas_call(
+        functools.partial(hidden_kernel, tp),
+        out_shape=[whole((row_count, model), bf16)]
+        + [whole((sp * capacity // blocks, model), bf16)] * blocks,
+        in_specs=[smem] + [vmem] * (4 + tp) + [hbm] * tp,
+        scratch_shapes=[VMEM((tp, depth, model), bf16), pltpu.SemaphoreType.DMA((tp,))],
+        cost_estimate=cost(flops=10**9, bytes_accessed=6 << 20),
+        name="hidden",
+    )(
+        place, norm_gain.reshape(tp, depth), residual, mix_gain.reshape(1, model), pick,
+        *parts, *[sources[k] for k in doubling(tp)],
     )
-    gathered_rows = returned.reshape(sp * capacity, -1)[target].reshape(row_count, PICKS, -1)
-    expert_mix = jnp.sum(route_weight[:, :, None] * gathered_rows.astype(f32), axis=1)
-    layer_out = layer_norm(deep_alpha * hidden.astype(f32) + expert_mix, final_gain)
-    return layer_out.astype(bf16)
+
+    weights = (expert_gate, expert_up, expert_down)
+    if relative:
+        half = sp // 2
+        order = list(range(half, sp)) + list(range(1, half))
+        came = {k: swap(outgoing[k], "sp", k) for k in order}
+        came[0] = outgoing[0]
+        back = {}
+        sets = [list(range(half)), list(range(half, half + half // 2)), list(range(half + half // 2, sp))]
+        for members in sets:
+            made = experts([came[k] for k in members], *weights)
+            for k, block in zip(members, made):
+                back[k] = swap(block, "sp", k) if k else block
+        returned = [back[k] for k in range(sp)]
+    else:
+        trade = functools.partial(
+            lax.all_to_all, axis_name="sp", split_axis=0, concat_axis=0, tiled=True
+        )
+        came = trade(outgoing[0].reshape(sp, capacity, model)).reshape(-1, model)
+        made = experts([came], *weights)[0]
+        returned = [trade(made.reshape(sp, capacity, model)).reshape(-1, model)]
+    return pl.pallas_call(
+        final_kernel,
+        out_shape=whole((row_count, model), bf16),
+        scratch_shapes=[VMEM((sp * capacity, model), bf16)],
+        cost_estimate=cost(flops=10**9, bytes_accessed=2 << 20),
+        name="final",
+    )(hidden, join, final_gain.reshape(1, model), *returned)
 
 
 def solution(mesh):

time: 133 us -> 97 us (0.73)
  the two profiles are of different devices: /device:TPU:0 before, /device:TPU:8 now
where the time goes in v2:
time: 97 us; the launch traced here: 96.7 us
  Pallas kernels  32.1 us (33%)
  waiting for transfers between devices  29.4 us (30%)
  starting transfers between devices  27.9 us (29%)
  local copies, waits for them, and re-layouts  5.68 us (6%)
  other arithmetic  1.39 us (1%)
    ppermute x23, waiting for transfers between devices, swap(): return lax.ppermute(value, axis, [(i, i ^ distance) for i in range(count)])  29.4 us
    ppermute x23, starting transfers between devices, swap(): return lax.ppermute(value, axis, [(i, i ^ distance) for i in range(count)])  27.9 us
    pallas_call x3, Pallas kernels, experts(): pl.pallas_call(functools.partial(expert_kernel, count), grid=(inner // ti...  13.7 us
    pallas_call x1, Pallas kernels, local(): pl.pallas_call(functools.partial(hidden_kernel, tp), out_shape=[whole((ro...  4.94 us
    pallas_call x1, Pallas kernels, local(): pl.pallas_call(read_kernel, out_shape=[whole((row_count, depth), bf16)] *...  4.48 us
    unnamed x53, local copies, waits for them, and re-layouts  4.36 us
    pallas_call x1, Pallas kernels, local(): pl.pallas_call(drive_kernel, out_shape=(whole((2, token_count, width)), w...  4.22 us
    pallas_call x1, Pallas kernels, local(): pl.pallas_call(final_kernel, out_shape=whole((row_count, model), bf16), s...  2.76 us
  transfers between devices with their start and end apart: 23, of which 11 were waited for; matrix products, arithmetic and copies ran while one was open for 4% of the time, Pallas kernels for 25%

profile of v2, /device:TPU:8, one launch (start us, length us, event | category | flops | bytes accessed | tf_op | source)
XLA Modules:
  0.0 96.7 jit_solution(4913677837926156666)
XLA Ops:
  0.0 1.5 %collective-permute-start.6 = (bf16[256,2048]{1,0:T(8,128)(2,1)}, bf16[256,2048]{1,0:T(8,128)(2,1)S(1)}, u32[]{:S(2)}, u32[]{:S(2)}) collective-permute-start(bf16[256,2048]{1,0:T(8,128)(2,1)} %rest_4_.1), channel_id=1, source_target_pairs={{0,2},{1,3},{2,0},{3,1},{4,6},{5,7},{6,4},{7,5},{8,10},{9,11},{10,... | collective-permute-start | bytes 3145736 | tf_op jit(solution)/shard_map/ppermute | solution.py:23
  1.5 4.2 %drive.1 = (f32[2,256,1024]{2,1,0:T(8,128)}, f32[256,1024]{1,0:T(8,128)}, f32[6,8,1024]{2,1,0:T(8,128)}, f32[1,4,1024]{2,1,0:T(4,128)}) custom-call(bf16[256,256]{1,0:T(8,128)(2,1)} %u_ref.3, f32[16,256]{1,0:T(8,128)} %held_ref.1, f32[16,64]{1,0:T(8,128)} %real_ref.1, f32[16,64]{1,0:T(8,128)} %freq_ref.1, f32[1,16]{1,0:T(1,128)} %bitcast.19, ...), custom_call_target="tpu_custom_call" | custom-call | flops 2000000000 | bytes 4194304 | tf_op jit(solution)/shard_map/drive/pallas_call | solution.py:403
  5.7 1.5 %collective-permute-start = (f32[1,4,1024]{2,1,0:T(4,128)}, f32[1,4,1024]{2,1,0:T(4,128)S(1)}, u32[]{:S(2)}, u32[]{:S(2)}) collective-permute-start(f32[1,4,1024]{2,1,0:T(4,128)} %get-tuple-element.35), channel_id=1, source_target_pairs={{0,4},{4,0},{8,12},{12,8},{16,20},{20,16},{24,28},{28,24},{1,5},{5... | collective-permute-start | bytes 49160 | tf_op jit(solution)/shard_map/ppermute | solution.py:23
  7.2 0.8 constant_dynamic-update-slice_fusion.2
  8.0 1.7 %collective-permute-done = f32[1,4,1024]{2,1,0:T(4,128)S(1)} collective-permute-done((f32[1,4,1024]{2,1,0:T(4,128)}, f32[1,4,1024]{2,1,0:T(4,128)S(1)}, u32[]{:S(2)}, u32[]{:S(2)}) %collective-permute-start) | collective-permute-done | bytes 16416 | tf_op jit(solution)/shard_map/ppermute | solution.py:23
  10.9 3.5 %collective-permute-done.1 = f32[2,4,1024]{2,1,0:T(4,128)S(1)} collective-permute-done((f32[2,4,1024]{2,1,0:T(4,128)S(1)}, f32[2,4,1024]{2,1,0:T(4,128)S(1)}, u32[]{:S(2)}, u32[]{:S(2)}) %collective-permute-start.1) | collective-permute-done | bytes 32800 | tf_op jit(solution)/shard_map/ppermute | solution.py:23
  14.4 2.7 %collective-permute-start.2 = (f32[4,4,1024]{2,1,0:T(4,128)S(1)}, f32[4,4,1024]{2,1,0:T(4,128)S(1)}, u32[]{:S(2)}, u32[]{:S(2)}) collective-permute-start(f32[4,4,1024]{2,1,0:T(4,128)S(1)} %constant_dynamic-update-slice_fusion.near_ref), channel_id=1, source_target_pairs={{0,16},{4,20},{8,24},{12,28},{16,0},{20,4},{24,8},{28,12},{1,17},{... | collective-permute-start | bytes 196616 | tf_op jit(solution)/shard_map/ppermute | solution.py:23
  17.7 1.9 %collective-permute-done.2.far_ref = f32[4,4,1024]{2,1,0:T(4,128)S(1)} collective-permute-done((f32[4,4,1024]{2,1,0:T(4,128)S(1)}, f32[4,4,1024]{2,1,0:T(4,128)S(1)}, u32[]{:S(2)}, u32[]{:S(2)}) %collective-permute-start.2) | collective-permute-done | bytes 65568 | tf_op jit(solution)/shard_map/ppermute | solution.py:23
  20.2 4.5 %readout.1 = (bf16[64,256]{1,0:T(8,128)(2,1)}, bf16[64,256]{1,0:T(8,128)(2,1)}, bf16[64,256]{1,0:T(8,128)(2,1)}, bf16[64,256]{1,0:T(8,128)(2,1)}) custom-call(s32[2]{0:T(128)} %pad_add_fusion.place_ref, bf16[256,256]{1,0:T(8,128)(2,1)} %u_ref.3, f32[2,256,1024]{2,1,0:T(8,128)} %get-tuple-element.38.drive_ref, f32[256,1024]{1,0:T(8,128)} %get-tuple-element.39.shrink_ref, ...), custom_call_target="tpu_custom_call" | custom-call | flops 2000000000 | bytes 4194304 | tf_op jit(solution)/shard_map/readout/pallas_call | solution.py:440
  25.3 1.3 %collective-permute-start.3 = (bf16[64,256]{1,0:T(8,128)(2,1)}, bf16[64,256]{1,0:T(8,128)(2,1)S(1)}, u32[]{:S(2)}, u32[]{:S(2)}) collective-permute-start(bf16[64,256]{1,0:T(8,128)(2,1)} %get-tuple-element.42), channel_id=1, source_target_pairs={{0,2},{1,3},{2,0},{3,1},{4,6},{5,7},{6,4},{7,5},{8,10},{9,11},{10,... | collective-permute-start | bytes 98312 | tf_op jit(solution)/shard_map/ppermute | solution.py:23
  29.5 2.0 %route.1 = (bf16[256,64]{1,0:T(8,128)(2,1)}, bf16[256,192]{1,0:T(8,128)(2,1)}) custom-call(s32[2]{0:T(128)} %pad_add_fusion.place_ref, s32[64,2]{1,0:T(8,128)} %copy.21.routes_ref, f32[64,2]{1,0:T(8,128)} %copy.22.weight_ref), custom_call_target="tpu_custom_call" | custom-call | flops 100000000 | bytes 131072 | tf_op jit(solution)/shard_map/route/pallas_call | solution.py:429
  32.5 4.9 %hidden.1 = (bf16[64,2048]{1,0:T(8,128)(2,1)}, bf16[32,2048]{1,0:T(8,128)(2,1)}, bf16[32,2048]{1,0:T(8,128)(2,1)}, bf16[32,2048]{1,0:T(8,128)(2,1)}, bf16[32,204...) custom-call(s32[2]{0:T(128)} %pad_add_fusion.place_ref, ...), custom_call_target="tpu_custom_call" | custom-call | flops 1000000000 | bytes 6291456 | tf_op jit(solution)/shard_map/hidden/pallas_call | solution.py:472
  37.4 1.6 %collective-permute-start.9 = (bf16[32,2048]{1,0:T(8,128)(2,1)}, bf16[32,2048]{1,0:T(8,128)(2,1)S(1)}, u32[]{:S(2)}, u32[]{:S(2)}) collective-permute-start(bf16[32,2048]{1,0:T(8,128)(2,1)} %get-tuple-element.50), channel_id=1, source_target_pairs={{0,4},{4,0},{8,12},{12,8},{16,20},{20,16},{24,28},{28,24},{1,5},{5... | collective-permute-start | bytes 393224 | tf_op jit(solution)/shard_map/ppermute | solution.py:23
  39.5 1.5 %collective-permute-start.11 = (bf16[32,2048]{1,0:T(8,128)(2,1)}, bf16[32,2048]{1,0:T(8,128)(2,1)S(1)}, u32[]{:S(2)}, u32[]{:S(2)}) collective-permute-start(bf16[32,2048]{1,0:T(8,128)(2,1)} %get-tuple-element.52), channel_id=1, source_target_pairs={{0,12},{4,8},{8,4},{12,0},{16,28},{20,24},{24,20},{28,16},{1,13},{... | collective-permute-start | bytes 393224 | tf_op jit(solution)/shard_map/ppermute | solution.py:23
  41.0 3.2 %collective-permute-start.15 = (bf16[32,2048]{1,0:T(8,128)(2,1)}, bf16[32,2048]{1,0:T(8,128)(2,1)S(1)}, u32[]{:S(2)}, u32[]{:S(2)}) collective-permute-start(bf16[32,2048]{1,0:T(8,128)(2,1)} %get-tuple-element.57), channel_id=1, source_target_pairs={{0,16},{4,20},{8,24},{12,28},{16,0},{20,4},{24,8},{28,12},{1,17},{... | collective-permute-start | bytes 393224 | tf_op jit(solution)/shard_map/ppermute | solution.py:23
  44.2 1.0 %collective-permute-start.16 = (bf16[32,2048]{1,0:T(8,128)(2,1)}, bf16[32,2048]{1,0:T(8,128)(2,1)S(1)}, u32[]{:S(2)}, u32[]{:S(2)}) collective-permute-start(bf16[32,2048]{1,0:T(8,128)(2,1)} %get-tuple-element.58), channel_id=1, source_target_pairs={{0,20},{4,16},{8,28},{12,24},{16,4},{20,0},{24,12},{28,8},{1,21},{... | collective-permute-start | bytes 393224 | tf_op jit(solution)/shard_map/ppermute | solution.py:23
  45.2 1.5 %collective-permute-start.19 = (bf16[32,2048]{1,0:T(8,128)(2,1)}, bf16[32,2048]{1,0:T(8,128)(2,1)S(1)}, u32[]{:S(2)}, u32[]{:S(2)}) collective-permute-start(bf16[32,2048]{1,0:T(8,128)(2,1)} %get-tuple-element.61), channel_id=1, source_target_pairs={{0,24},{4,28},{8,16},{12,20},{16,8},{20,12},{24,0},{28,4},{1,25},{... | collective-permute-start | bytes 393224 | tf_op jit(solution)/shard_map/ppermute | solution.py:23
  46.6 1.1 %collective-permute-done.10.rest_2_ = bf16[32,2048]{1,0:T(8,128)(2,1)S(1)} collective-permute-done((bf16[32,2048]{1,0:T(8,128)(2,1)}, bf16[32,2048]{1,0:T(8,128)(2,1)S(1)}, u32[]{:S(2)}, u32[]{:S(2)}) %collective-permute-start.10) | collective-permute-done | bytes 131104 | tf_op jit(solution)/shard_map/ppermute | solution.py:23
  47.8 2.1 %collective-permute-done.11.rest_3_ = bf16[32,2048]{1,0:T(8,128)(2,1)S(1)} collective-permute-done((bf16[32,2048]{1,0:T(8,128)(2,1)}, bf16[32,2048]{1,0:T(8,128)(2,1)S(1)}, u32[]{:S(2)}, u32[]{:S(2)}) %collective-permute-start.11) | collective-permute-done | bytes 131104 | tf_op jit(solution)/shard_map/ppermute | solution.py:23
  50.5 4.7 %experts.3 = (bf16[32,2048]{1,0:T(8,128)(2,1)}, bf16[32,2048]{1,0:T(8,128)(2,1)}, bf16[32,2048]{1,0:T(8,128)(2,1)}, bf16[32,2048]{1,0:T(8,128)(2,1)}) custom-call(bf16[1,2048,512]{2,1,0:T(8,128)(2,1)} %gate_ref.5, bf16[1,2048,512]{2,1,0:T(8,128)(2,1)} %up_ref.5, bf16[1,512,2048]{2,1,0:T(8,128)(2,1)} %down_ref.5, bf16[32,2048]{1,0:T(8,128)(2,1)} %get-tuple-element.49.rest_0_, ...), custom_call_target="tpu_custom_call" | custom-call | flops 1000000000 | bytes 6291456 | tf_op jit(solution)/shard_map/experts/pallas_call | solution.py:354
  55.2 1.1 %collective-permute-start.12 = (bf16[32,2048]{1,0:T(8,128)(2,1)}, bf16[32,2048]{1,0:T(8,128)(2,1)S(1)}, u32[]{:S(2)}, u32[]{:S(2)}) collective-permute-start(bf16[32,2048]{1,0:T(8,128)(2,1)} %get-tuple-element.54), channel_id=1, source_target_pairs={{0,4},{4,0},{8,12},{12,8},{16,20},{20,16},{24,28},{28,24},{1,5},{5... | collective-permute-start | bytes 393224 | tf_op jit(solution)/shard_map/ppermute | solution.py:23
  56.2 3.1 %collective-permute-done.15.rest_0_ = bf16[32,2048]{1,0:T(8,128)(2,1)S(1)} collective-permute-done((bf16[32,2048]{1,0:T(8,128)(2,1)}, bf16[32,2048]{1,0:T(8,128)(2,1)S(1)}, u32[]{:S(2)}, u32[]{:S(2)}) %collective-permute-start.15) | collective-permute-done | bytes 131104 | tf_op jit(solution)/shard_map/ppermute | solution.py:23
  59.7 2.5 %collective-permute-done.16.rest_1_ = bf16[32,2048]{1,0:T(8,128)(2,1)S(1)} collective-permute-done((bf16[32,2048]{1,0:T(8,128)(2,1)}, bf16[32,2048]{1,0:T(8,128)(2,1)S(1)}, u32[]{:S(2)}, u32[]{:S(2)}) %collective-permute-start.16) | collective-permute-done | bytes 131104 | tf_op jit(solution)/shard_map/ppermute | solution.py:23
  62.2 2.3 %collective-permute-start.14 = (bf16[32,2048]{1,0:T(8,128)(2,1)}, bf16[32,2048]{1,0:T(8,128)(2,1)S(1)}, u32[]{:S(2)}, u32[]{:S(2)}) collective-permute-start(bf16[32,2048]{1,0:T(8,128)(2,1)} %get-tuple-element.56), channel_id=1, source_target_pairs={{0,12},{4,8},{8,4},{12,0},{16,28},{20,24},{24,20},{28,16},{1,13},{... | collective-permute-start | bytes 393224 | tf_op jit(solution)/shard_map/ppermute | solution.py:23
  64.5 4.5 %experts.4 = (bf16[32,2048]{1,0:T(8,128)(2,1)}, bf16[32,2048]{1,0:T(8,128)(2,1)}) custom-call(bf16[1,2048,512]{2,1,0:T(8,128)(2,1)} %gate_ref.5, bf16[1,2048,512]{2,1,0:T(8,128)(2,1)} %up_ref.5, bf16[1,512,2048]{2,1,0:T(8,128)(2,1)} %down_ref.5, bf16[32,2048]{1,0:T(8,128)(2,1)} %copy-done.5, bf16[32,2048]{1,0:T(8,128)(2,1)} %copy-done.6), custom_call_target="tpu_custom_call" | custom-call | flops 1000000000 | bytes 6291456 | tf_op jit(solution)/shard_map/experts/pallas_call | solution.py:354
  69.0 2.2 %collective-permute-start.17 = (bf16[32,2048]{1,0:T(8,128)(2,1)}, bf16[32,2048]{1,0:T(8,128)(2,1)S(1)}, u32[]{:S(2)}, u32[]{:S(2)}) collective-permute-start(bf16[32,2048]{1,0:T(8,128)(2,1)} %get-tuple-element.59), channel_id=1, source_target_pairs={{0,16},{4,20},{8,24},{12,28},{16,0},{20,4},{24,8},{28,12},{1,17},{... | collective-permute-start | bytes 393224 | tf_op jit(solution)/shard_map/ppermute | solution.py:23
  71.8 4.5 %experts.5 = (bf16[32,2048]{1,0:T(8,128)(2,1)}, bf16[32,2048]{1,0:T(8,128)(2,1)}) custom-call(bf16[1,2048,512]{2,1,0:T(8,128)(2,1)} %gate_ref.5, bf16[1,2048,512]{2,1,0:T(8,128)(2,1)} %up_ref.5, bf16[1,512,2048]{2,1,0:T(8,128)(2,1)} %down_ref.5, bf16[32,2048]{1,0:T(8,128)(2,1)} %copy-done.3, bf16[32,2048]{1,0:T(8,128)(2,1)} %copy-done.4), custom_call_target="tpu_custom_call" | custom-call | flops 1000000000 | bytes 6291456 | tf_op jit(solution)/shard_map/experts/pallas_call | solution.py:354
  76.4 3.1 %collective-permute-start.21 = (bf16[32,2048]{1,0:T(8,128)(2,1)}, bf16[32,2048]{1,0:T(8,128)(2,1)S(1)}, u32[]{:S(2)}, u32[]{:S(2)}) collective-permute-start(bf16[32,2048]{1,0:T(8,128)(2,1)} %get-tuple-element.63), channel_id=1, source_target_pairs={{0,24},{4,28},{8,16},{12,20},{16,8},{20,12},{24,0},{28,4},{1,25},{... | collective-permute-start | bytes 393224 | tf_op jit(solution)/shard_map/ppermute | solution.py:23
  80.1 6.6 %collective-permute-done.18.rest_5_ = bf16[32,2048]{1,0:T(8,128)(2,1)S(1)} collective-permute-done((bf16[32,2048]{1,0:T(8,128)(2,1)}, bf16[32,2048]{1,0:T(8,128)(2,1)S(1)}, u32[]{:S(2)}, u32[]{:S(2)}) %collective-permute-start.18) | collective-permute-done | bytes 131104 | tf_op jit(solution)/shard_map/ppermute | solution.py:23
  86.6 3.6 %collective-permute-done.21.rest_6_ = bf16[32,2048]{1,0:T(8,128)(2,1)S(1)} collective-permute-done((bf16[32,2048]{1,0:T(8,128)(2,1)}, bf16[32,2048]{1,0:T(8,128)(2,1)S(1)}, u32[]{:S(2)}, u32[]{:S(2)}) %collective-permute-start.21) | collective-permute-done | bytes 131104 | tf_op jit(solution)/shard_map/ppermute | solution.py:23
  90.2 3.1 %collective-permute-done.22.rest_7_ = bf16[32,2048]{1,0:T(8,128)(2,1)S(1)} collective-permute-done((bf16[32,2048]{1,0:T(8,128)(2,1)}, bf16[32,2048]{1,0:T(8,128)(2,1)S(1)}, u32[]{:S(2)}, u32[]{:S(2)}) %collective-permute-start.22) | collective-permute-done | bytes 131104 | tf_op jit(solution)/shard_map/ppermute | solution.py:23
  93.9 2.8 %final.1 = bf16[64,2048]{1,0:T(8,128)(2,1)} custom-call(bf16[64,2048]{1,0:T(8,128)(2,1)} %get-tuple-element.47.hidden_ref, bf16[256,192]{1,0:T(8,128)(2,1)} %get-tuple-element.48.join_ref, f32[1,2048]{1,0:T(1,128)} %bitcast.18, bf16[32,2048]{1,0:T(8,128)(2,1)} %get-tuple-element.53.rest_0_, bf16[32,2048]{1,0:T(8,128)(2,1)} %copy-done.17, ...), custom_call_target="tpu_custom_call" | custom-call | flops 1000000000 | bytes 2097152 | tf_op jit(solution)/shard_map/final/pallas_call | solution.py:505
  (80 shorter events, 10.2 us)
Async XLA Ops:
  0.0 25.1 %collective-permute-start.6 = (bf16[256,2048]{1,0:T(8,128)(2,1)}, bf16[256,2048]{1,0:T(8,128)(2,1)S(1)}, u32[]{:S(2)}, u32[]{:S(2)}) collective-permute-start(bf16[256,2048]{1,0:T(8,128)(2,1)} %rest_4_.1), channel_id=1, source_target_pairs={{0,2},{1,3},{2,0},{3,1},{4,6},{5,7},{6,4},{7,5},{8,10},{9,11},{10,... | collective-permute-start | bytes 3145736 | tf_op jit(solution)/shard_map/ppermute | solution.py:23
  5.7 3.9 %collective-permute-start = (f32[1,4,1024]{2,1,0:T(4,128)}, f32[1,4,1024]{2,1,0:T(4,128)S(1)}, u32[]{:S(2)}, u32[]{:S(2)}) collective-permute-start(f32[1,4,1024]{2,1,0:T(4,128)} %get-tuple-element.35), channel_id=1, source_target_pairs={{0,4},{4,0},{8,12},{12,8},{16,20},{20,16},{24,28},{28,24},{1,5},{5... | collective-permute-start | bytes 49160 | tf_op jit(solution)/shard_map/ppermute | solution.py:23
  10.4 4.0 %collective-permute-start.1 = (f32[2,4,1024]{2,1,0:T(4,128)S(1)}, f32[2,4,1024]{2,1,0:T(4,128)S(1)}, u32[]{:S(2)}, u32[]{:S(2)}) collective-permute-start(f32[2,4,1024]{2,1,0:T(4,128)S(1)} %pad_maximum_fusion), channel_id=1, source_target_pairs={{0,8},{4,12},{8,0},{12,4},{16,24},{20,28},{24,16},{28,20},{1,9},{5... | collective-permute-start | bytes 98312 | tf_op jit(solution)/shard_map/ppermute | solution.py:23
  14.4 5.2 %collective-permute-start.2 = (f32[4,4,1024]{2,1,0:T(4,128)S(1)}, f32[4,4,1024]{2,1,0:T(4,128)S(1)}, u32[]{:S(2)}, u32[]{:S(2)}) collective-permute-start(f32[4,4,1024]{2,1,0:T(4,128)S(1)} %constant_dynamic-update-slice_fusion.near_ref), channel_id=1, source_target_pairs={{0,16},{4,20},{8,24},{12,28},{16,0},{20,4},{24,8},{28,12},{1,17},{... | collective-permute-start | bytes 196616 | tf_op jit(solution)/shard_map/ppermute | solution.py:23
  20.2 7.2 %copy-start.14 = (f32[1024]{0:T(1024)S(1)}, f32[1024]{0:T(1024)}, u32[]{:S(2)}) copy-start(f32[1024]{0:T(1024)} %param.30) | copy-start | bytes 12292
  20.2 7.8 %copy-start.15 = (f32[64,2]{0,1:T(2,128)S(1)}, f32[64,2]{0,1:T(2,128)}, u32[]{:S(2)}) copy-start(f32[64,2]{0,1:T(2,128)} %param.35) | copy-start | bytes 1540
  20.2 8.5 %copy-start.16 = (s32[64,2]{0,1:T(2,128)S(1)}, s32[64,2]{0,1:T(2,128)}, u32[]{:S(2)}) copy-start(s32[64,2]{0,1:T(2,128)} %param.34) | copy-start | bytes 1540
  24.7 6.8 %collective-permute-start.7 = (bf16[256,2048]{1,0:T(8,128)(2,1)S(1)}, bf16[256,2048]{1,0:T(8,128)(2,1)S(1)}, u32[]{:S(2)}, u32[]{:S(2)}) collective-permute-start(bf16[256,2048]{1,0:T(8,128)(2,1)S(1)} %copy-done), channel_id=1, source_target_pairs={{0,1},{1,0},{2,3},{3,2},{4,5},{5,4},{6,7},{7,6},{8,9},{9,8},{10,11... | collective-permute-start | bytes 3145736 | tf_op jit(solution)/shard_map/ppermute | solution.py:23
  25.1 6.4 %copy-start.1 = (bf16[256,2048]{1,0:T(8,128)(2,1)}, bf16[256,2048]{1,0:T(8,128)(2,1)S(1)}, u32[]{:S(2)}) copy-start(bf16[256,2048]{1,0:T(8,128)(2,1)S(1)} %collective-permute-done.6.rest_5_) | copy-start | bytes 3145732
  25.1 6.4 %collective-permute-start.8 = (bf16[256,2048]{1,0:T(8,128)(2,1)S(1)}, bf16[256,2048]{1,0:T(8,128)(2,1)}, u32[]{:S(2)}, u32[]{:S(2)}) collective-permute-start(bf16[256,2048]{1,0:T(8,128)(2,1)S(1)} %collective-permute-done.6.rest_5_), channel_id=1, source_target_pairs={{0,1},{1,0},{2,3},{3,2},{4,5},{5,4},{6,7},{7,6},{8,9},{9,8},{10,11... | collective-permute-start | bytes 3145736 | tf_op jit(solution)/shard_map/ppermute | solution.py:23
  25.3 6.2 %collective-permute-start.3 = (bf16[64,256]{1,0:T(8,128)(2,1)}, bf16[64,256]{1,0:T(8,128)(2,1)S(1)}, u32[]{:S(2)}, u32[]{:S(2)}) collective-permute-start(bf16[64,256]{1,0:T(8,128)(2,1)} %get-tuple-element.42), channel_id=1, source_target_pairs={{0,2},{1,3},{2,0},{3,1},{4,6},{5,7},{6,4},{7,5},{8,10},{9,11},{10,... | collective-permute-start | bytes 98312 | tf_op jit(solution)/shard_map/ppermute | solution.py:23
  26.6 4.9 %collective-permute-start.4 = (bf16[64,256]{1,0:T(8,128)(2,1)}, bf16[64,256]{1,0:T(8,128)(2,1)S(1)}, u32[]{:S(2)}, u32[]{:S(2)}) collective-permute-start(bf16[64,256]{1,0:T(8,128)(2,1)} %get-tuple-element.43), channel_id=1, source_target_pairs={{0,1},{1,0},{2,3},{3,2},{4,5},{5,4},{6,7},{7,6},{8,9},{9,8},{10,11... | collective-permute-start | bytes 98312 | tf_op jit(solution)/shard_map/ppermute | solution.py:23
  26.8 4.7 %collective-permute-start.5 = (bf16[64,256]{1,0:T(8,128)(2,1)}, bf16[64,256]{1,0:T(8,128)(2,1)S(1)}, u32[]{:S(2)}, u32[]{:S(2)}) collective-permute-start(bf16[64,256]{1,0:T(8,128)(2,1)} %get-tuple-element.44), channel_id=1, source_target_pairs={{0,3},{1,2},{2,1},{3,0},{4,7},{5,6},{6,5},{7,4},{8,11},{9,10},{10,... | collective-permute-start | bytes 98312 | tf_op jit(solution)/shard_map/ppermute | solution.py:23
  37.4 7.7 %collective-permute-start.9 = (bf16[32,2048]{1,0:T(8,128)(2,1)}, bf16[32,2048]{1,0:T(8,128)(2,1)S(1)}, u32[]{:S(2)}, u32[]{:S(2)}) collective-permute-start(bf16[32,2048]{1,0:T(8,128)(2,1)} %get-tuple-element.50), channel_id=1, source_target_pairs={{0,4},{4,0},{8,12},{12,8},{16,20},{20,16},{24,28},{28,24},{1,5},{5... | collective-permute-start | bytes 393224 | tf_op jit(solution)/shard_map/ppermute | solution.py:23
  39.0 8.7 %collective-permute-start.10 = (bf16[32,2048]{1,0:T(8,128)(2,1)}, bf16[32,2048]{1,0:T(8,128)(2,1)S(1)}, u32[]{:S(2)}, u32[]{:S(2)}) collective-permute-start(bf16[32,2048]{1,0:T(8,128)(2,1)} %get-tuple-element.51), channel_id=1, source_target_pairs={{0,8},{4,12},{8,0},{12,4},{16,24},{20,28},{24,16},{28,20},{1,9},{5... | collective-permute-start | bytes 393224 | tf_op jit(solution)/shard_map/ppermute | solution.py:23
  39.5 10.4 %collective-permute-start.11 = (bf16[32,2048]{1,0:T(8,128)(2,1)}, bf16[32,2048]{1,0:T(8,128)(2,1)S(1)}, u32[]{:S(2)}, u32[]{:S(2)}) collective-permute-start(bf16[32,2048]{1,0:T(8,128)(2,1)} %get-tuple-element.52), channel_id=1, source_target_pairs={{0,12},{4,8},{8,4},{12,0},{16,28},{20,24},{24,20},{28,16},{1,13},{... | collective-permute-start | bytes 393224 | tf_op jit(solution)/shard_map/ppermute | solution.py:23
  41.0 18.4 %collective-permute-start.15 = (bf16[32,2048]{1,0:T(8,128)(2,1)}, bf16[32,2048]{1,0:T(8,128)(2,1)S(1)}, u32[]{:S(2)}, u32[]{:S(2)}) collective-permute-start(bf16[32,2048]{1,0:T(8,128)(2,1)} %get-tuple-element.57), channel_id=1, source_target_pairs={{0,16},{4,20},{8,24},{12,28},{16,0},{20,4},{24,8},{28,12},{1,17},{... | collective-permute-start | bytes 393224 | tf_op jit(solution)/shard_map/ppermute | solution.py:23
  44.2 18.0 %collective-permute-start.16 = (bf16[32,2048]{1,0:T(8,128)(2,1)}, bf16[32,2048]{1,0:T(8,128)(2,1)S(1)}, u32[]{:S(2)}, u32[]{:S(2)}) collective-permute-start(bf16[32,2048]{1,0:T(8,128)(2,1)} %get-tuple-element.58), channel_id=1, source_target_pairs={{0,20},{4,16},{8,28},{12,24},{16,4},{20,0},{24,12},{28,8},{1,21},{... | collective-permute-start | bytes 393224 | tf_op jit(solution)/shard_map/ppermute | solution.py:23
  45.2 23.8 %collective-permute-start.19 = (bf16[32,2048]{1,0:T(8,128)(2,1)}, bf16[32,2048]{1,0:T(8,128)(2,1)S(1)}, u32[]{:S(2)}, u32[]{:S(2)}) collective-permute-start(bf16[32,2048]{1,0:T(8,128)(2,1)} %get-tuple-element.61), channel_id=1, source_target_pairs={{0,24},{4,28},{8,16},{12,20},{16,8},{20,12},{24,0},{28,4},{1,25},{... | collective-permute-start | bytes 393224 | tf_op jit(solution)/shard_map/ppermute | solution.py:23
  47.8 23.4 %collective-permute-start.20 = (bf16[32,2048]{1,0:T(8,128)(2,1)}, bf16[32,2048]{1,0:T(8,128)(2,1)S(1)}, u32[]{:S(2)}, u32[]{:S(2)}) collective-permute-start(bf16[32,2048]{1,0:T(8,128)(2,1)} %get-tuple-element.62), channel_id=1, source_target_pairs={{0,28},{4,24},{8,20},{12,16},{16,12},{20,8},{24,4},{28,0},{1,29},{... | collective-permute-start | bytes 393224 | tf_op jit(solution)/shard_map/ppermute | solution.py:23
  55.2 21.2 %collective-permute-start.12 = (bf16[32,2048]{1,0:T(8,128)(2,1)}, bf16[32,2048]{1,0:T(8,128)(2,1)S(1)}, u32[]{:S(2)}, u32[]{:S(2)}) collective-permute-start(bf16[32,2048]{1,0:T(8,128)(2,1)} %get-tuple-element.54), channel_id=1, source_target_pairs={{0,4},{4,0},{8,12},{12,8},{16,20},{20,16},{24,28},{28,24},{1,5},{5... | collective-permute-start | bytes 393224 | tf_op jit(solution)/shard_map/ppermute | solution.py:23
  59.4 20.1 %collective-permute-start.13 = (bf16[32,2048]{1,0:T(8,128)(2,1)}, bf16[32,2048]{1,0:T(8,128)(2,1)S(1)}, u32[]{:S(2)}, u32[]{:S(2)}) collective-permute-start(bf16[32,2048]{1,0:T(8,128)(2,1)} %get-tuple-element.55), channel_id=1, source_target_pairs={{0,8},{4,12},{8,0},{12,4},{16,24},{20,28},{24,16},{28,20},{1,9},{5... | collective-permute-start | bytes 393224 | tf_op jit(solution)/shard_map/ppermute | solution.py:23
  62.2 17.9 %collective-permute-start.14 = (bf16[32,2048]{1,0:T(8,128)(2,1)}, bf16[32,2048]{1,0:T(8,128)(2,1)S(1)}, u32[]{:S(2)}, u32[]{:S(2)}) collective-permute-start(bf16[32,2048]{1,0:T(8,128)(2,1)} %get-tuple-element.56), channel_id=1, source_target_pairs={{0,12},{4,8},{8,4},{12,0},{16,28},{20,24},{24,20},{28,16},{1,13},{... | collective-permute-start | bytes 393224 | tf_op jit(solution)/shard_map/ppermute | solution.py:23
  69.0 11.1 %collective-permute-start.17 = (bf16[32,2048]{1,0:T(8,128)(2,1)}, bf16[32,2048]{1,0:T(8,128)(2,1)S(1)}, u32[]{:S(2)}, u32[]{:S(2)}) collective-permute-start(bf16[32,2048]{1,0:T(8,128)(2,1)} %get-tuple-element.59), channel_id=1, source_target_pairs={{0,16},{4,20},{8,24},{12,28},{16,0},{20,4},{24,8},{28,12},{1,17},{... | collective-permute-start | bytes 393224 | tf_op jit(solution)/shard_map/ppermute | solution.py:23
  71.2 15.5 %collective-permute-start.18 = (bf16[32,2048]{1,0:T(8,128)(2,1)}, bf16[32,2048]{1,0:T(8,128)(2,1)S(1)}, u32[]{:S(2)}, u32[]{:S(2)}) collective-permute-start(bf16[32,2048]{1,0:T(8,128)(2,1)} %get-tuple-element.60), channel_id=1, source_target_pairs={{0,20},{4,16},{8,28},{12,24},{16,4},{20,0},{24,12},{28,8},{1,21},{... | collective-permute-start | bytes 393224 | tf_op jit(solution)/shard_map/ppermute | solution.py:23
  76.4 16.9 %copy-start.17 = (bf16[32,2048]{1,0:T(8,128)(2,1)}, bf16[32,2048]{1,0:T(8,128)(2,1)S(1)}, u32[]{:S(2)}) copy-start(bf16[32,2048]{1,0:T(8,128)(2,1)S(1)} %collective-permute-done.12.rest_1_) | copy-start | bytes 393220
  76.4 13.8 %collective-permute-start.21 = (bf16[32,2048]{1,0:T(8,128)(2,1)}, bf16[32,2048]{1,0:T(8,128)(2,1)S(1)}, u32[]{:S(2)}, u32[]{:S(2)}) collective-permute-start(bf16[32,2048]{1,0:T(8,128)(2,1)} %get-tuple-element.63), channel_id=1, source_target_pairs={{0,24},{4,28},{8,16},{12,20},{16,8},{20,12},{24,0},{28,4},{1,25},{... | collective-permute-start | bytes 393224 | tf_op jit(solution)/shard_map/ppermute | solution.py:23
  79.5 13.8 %copy-start.18 = (bf16[32,2048]{1,0:T(8,128)(2,1)}, bf16[32,2048]{1,0:T(8,128)(2,1)S(1)}, u32[]{:S(2)}) copy-start(bf16[32,2048]{1,0:T(8,128)(2,1)S(1)} %collective-permute-done.13.rest_2_) | copy-start | bytes 393220
  79.5 13.8 %collective-permute-start.22 = (bf16[32,2048]{1,0:T(8,128)(2,1)}, bf16[32,2048]{1,0:T(8,128)(2,1)S(1)}, u32[]{:S(2)}, u32[]{:S(2)}) collective-permute-start(bf16[32,2048]{1,0:T(8,128)(2,1)} %get-tuple-element.64), channel_id=1, source_target_pairs={{0,28},{4,24},{8,20},{12,16},{16,12},{20,8},{24,4},{28,0},{1,29},{... | collective-permute-start | bytes 393224 | tf_op jit(solution)/shard_map/ppermute | solution.py:23
  80.0 13.2 %copy-start.19 = (bf16[32,2048]{1,0:T(8,128)(2,1)}, bf16[32,2048]{1,0:T(8,128)(2,1)S(1)}, u32[]{:S(2)}) copy-start(bf16[32,2048]{1,0:T(8,128)(2,1)S(1)} %collective-permute-done.14.rest_3_) | copy-start | bytes 393220
  80.0 13.2 %copy-start.20 = (bf16[32,2048]{1,0:T(8,128)(2,1)}, bf16[32,2048]{1,0:T(8,128)(2,1)S(1)}, u32[]{:S(2)}) copy-start(bf16[32,2048]{1,0:T(8,128)(2,1)S(1)} %collective-permute-done.17.rest_4_) | copy-start | bytes 393220
  86.6 6.7 %copy-start.21 = (bf16[32,2048]{1,0:T(8,128)(2,1)}, bf16[32,2048]{1,0:T(8,128)(2,1)S(1)}, u32[]{:S(2)}) copy-start(bf16[32,2048]{1,0:T(8,128)(2,1)S(1)} %collective-permute-done.18.rest_5_) | copy-start | bytes 393220
  (16 other events, 35.3 us)
